TPU v7x, 256 devices: a whole 4x4x8 slice. The times are simulated.
256 devices in a mesh: sp: 64 (over z, y, core), tp: 4 (over x).
Axes of the slice: x: 4, y: 4, z: 8, core: 2. Of those that a mesh axis runs over, the one named last changes fastest.
Arguments:
- out_grad: bfloat16 [8192, 2048], P('sp'), may hold values from -16 to 16
- residual: bfloat16 [8192, 2048], P('sp'), may hold values from -6 to 6
- routes: int32 [8192, 2], P('sp'), may hold values from 0 to 31, all different within a row; in each aligned block of 128 rows (0 to 127, 128 to 255, ...) at most 10 rows name the same one
- route_weights: float32 [8192, 2], P('sp'), may hold values from 0.15 to 0.85, as said below
- w_gate: bfloat16 [64, 2048, 2048], P('sp', None, 'tp'), may hold values from -0.125 to 0.125
- w_up: bfloat16 [64, 2048, 2048], P('sp', None, 'tp'), may hold values from -0.125 to 0.125
- w_down: bfloat16 [64, 2048, 2048], P('sp', 'tp'), may hold values from -0.09375 to 0.09375
- out_gate: bfloat16 [8192, 1024], P('sp', 'tp'), may hold values from -6 to 6
- in_gate: bfloat16 [8192, 1024], P('sp', 'tp'), may hold values from -6 to 6
- conv_input: bfloat16 [8192, 1024], P('sp', 'tp'), may hold values from -6 to 6
- conv_out: bfloat16 [8192, 1024], P('sp', 'tp'), may hold values from -6 to 6
- conv_taps: float32 [3, 1024], P(None, 'tp'), may hold values from -3.5 to 3.5
- w_out: bfloat16 [1024, 2048], P('tp'), may hold values from -0.1875 to 0.1875
Outputs:
- grad_resid: bfloat16 [8192, 2048], P('sp')
- grad_up: bfloat16 [64, 2048, 2048], P('sp', None, 'tp')
- grad_down: bfloat16 [64, 2048, 2048], P('sp', 'tp')
- grad_out_gate: bfloat16 [8192, 1024], P('sp', 'tp')
- grad_in_gate: bfloat16 [8192, 1024], P('sp', 'tp')
- grad_conv_input: bfloat16 [8192, 1024], P('sp', 'tp')
- grad_w_out: float32 [2048, 1024], P('sp', 'tp')
Inputs may be any that keep to these rules, and one draw needn't show every extreme that they name: `routes`: each row names 2 different experts. In the rows of one index of sp no expert is named more than 10 times, a bound that some block reaches. `route_weights`: the two weights of a row sum to one.
All inputs are finite; a program needn't handle non-finite values.
Results may differ from a plain program's by a relative error of at most 0.013.
Values may be sent and summed in bfloat16 or wider, within the bound.
A program may use at most 128 MiB of HBM per device.

v0:
```python
import jax
import jax.numpy as jnp
import numpy as np
from jax import lax
from jax.experimental import pallas as pl
from jax.experimental.pallas import tpu as pltpu
from jax.sharding import PartitionSpec as P

MESH = pl.DeviceIdType.MESH
EPS = 1e-06
F32 = jnp.float32
BF16 = jnp.bfloat16

D = 2048
H = 512
Q = 512
TOK = 128
CAP = 10
NZ, NY, NX = 8, 4, 4
CHIPS = NZ * NY
MSG = 4 * CAP
GROUPS = 4
GROW = 8 * CAP
HALF = GROUPS * GROW
C = 256
Z_ORDER = (0, 1, 7, 2, 6, 3, 5, 4)
O_OFF = (2, 1, 3, 0)


def permutation():
    place = np.zeros((8 * MSG, 8 * MSG), np.float32)
    for part in range(4):
        for source in range(8):
            for slot in range(CAP):
                place[part * GROW + source * CAP + slot, source * MSG + part * CAP + slot] = 1
    return place


def nt(a, b):
    return lax.dot_general(a, b, (((1,), (1,)), ((), ())), preferred_element_type=F32)


def tn(a, b):
    return lax.dot_general(a, b, (((0,), (0,)), ((), ())), preferred_element_type=F32)


def nn(a, b):
    return jnp.dot(a, b, preferred_element_type=F32)


def m8(value, by=8):
    return pl.multiple_of(value, by)


def kernel(
    og, resid, routes, rw, wg_h, wu_h, wd_h, ogate, igate, cin, cout, taps, wout, perm, perm_t,
    gr_o, gup_o, gdn_o, gog_o, gig_o, gci_o, gwo_o,
    wg, wu, wd, s_buf, r_buf, xa, hid, dga, dup, ps, pr, po, ra, rb, rc, rd, cs, rt, bk, dn,
    gacc, gb, gp, gs, g_in, dcv, hp, hn, gup, gdn,
    w_sem, loc_sem, pl_s, pl_r, rt_s, rt_r, g_s, g_r, xs, xr, q_s, q_r, e_s, e_r, dn_s, dn_r, t_s, t_r, out_sem,
):
    s = lax.axis_index("sp")
    x = lax.axis_index("tp")
    c = s // 2
    k = s % 2
    z = c // NY
    y = c % NY
    right = (s, (x + 1) % NX)
    left = (s, (x + 3) % NX)
    mate = (2 * c + 1 - k, x)
    before = ((s + 63) % 64, x)
    after = ((s + 1) % 64, x)
    across = ((s + 63 + 2 * k) % 64, x)

    def expert_of(i, dy):
        return ((z + NZ - Z_ORDER[i]) % NZ) * NY + (y + dy) % NY

    def source_of(p):
        return ((z + Z_ORDER[p // NY]) % NZ) * NY + (y + p % NY) % NY

    def place_of(i, dy):
        return i * NY + (NY - dy) % NY

    def rcopy(src, dst, ss, rs, dev):
        return pltpu.make_async_remote_copy(
            src_ref=src, dst_ref=dst, send_sem=ss, recv_sem=rs, device_id=dev, device_id_type=MESH
        )

    barrier = pltpu.get_barrier_semaphore()
    for i in range(NZ):
        for dy in range(NY):
            if i or dy:
                pl.semaphore_signal(
                    barrier, inc=1, device_id=(2 * expert_of(i, dy) + k, x), device_id_type=MESH
                )
    for dev in (right, left, mate, across):
        pl.semaphore_signal(barrier, inc=1, device_id=dev, device_id_type=MESH)

    w_copies = [
        pltpu.make_async_copy(wg_h.at[0], wg, w_sem.at[0]),
        pltpu.make_async_copy(wu_h.at[0], wu, w_sem.at[1]),
        pltpu.make_async_copy(wd_h.at[0], wd, w_sem.at[2]),
    ]
    for copy in w_copies:
        copy.start()

    lanes = lax.broadcasted_iota(jnp.int32, (TOK, TOK), 1)
    subs = lax.broadcasted_iota(jnp.int32, (TOK, TOK), 0)
    r0 = routes[:, 0:1]
    r1 = routes[:, 1:2]
    a0 = (lanes == r0).astype(F32)
    a1 = (lanes == r1).astype(F32)
    earlier = (lanes < subs).astype(F32).astype(BF16)
    counts = nn(earlier, (a0 + a1).astype(BF16))
    s0 = r0.astype(F32) * MSG + jnp.sum(a0 * counts, axis=1, keepdims=True)
    s1 = r1.astype(F32) * MSG + jnp.sum(a1 * counts, axis=1, keepdims=True)
    eye = lanes == subs
    s0_row = jnp.sum(jnp.where(eye, s0, 0.0), axis=0, keepdims=True)
    s1_row = jnp.sum(jnp.where(eye, s1, 0.0), axis=0, keepdims=True)

    rf = resid[...].astype(F32)
    inv = lax.rsqrt(jnp.mean(rf * rf, axis=-1, keepdims=True) + EPS)
    qcol = m8(x * Q, Q)
    norm_q = (resid[:, pl.ds(qcol, Q)].astype(F32) * inv).astype(BF16)
    og_q = og[:, pl.ds(qcol, Q)].astype(F32)
    w0_q = (rw[:, 0:1] * og_q).astype(BF16)
    w1_q = (rw[:, 1:2] * og_q).astype(BF16)
    data = jnp.concatenate(
        [
            norm_q[:, :256], norm_q[:, 256:],
            w0_q[:, :256], w1_q[:, :256], w0_q[:, 256:], w1_q[:, 256:],
        ],
        axis=0,
    )

    def build(b, carry):
        rows = (lax.broadcasted_iota(jnp.int32, (8 * MSG, TOK), 0) + b * (8 * MSG)).astype(F32)

        def hot(base):
            return (rows == base).astype(F32)

        picks = jnp.concatenate(
            [
                hot(s0_row) + hot(s1_row),
                hot(s0_row + CAP) + hot(s1_row + CAP),
                hot(s0_row + 2 * CAP), hot(s1_row + 2 * CAP),
                hot(s0_row + 3 * CAP), hot(s1_row + 3 * CAP),
            ],
            axis=1,
        ).astype(BF16)
        s_buf[pl.ds(m8(b * 8 * MSG, 8 * MSG), 8 * MSG), :] = nn(picks, data).astype(BF16)
        return carry

    lax.fori_loop(0, GROUPS, build, 0)

    pl.semaphore_wait(barrier, 35)

    def send_rows(i, dy):
        e = expert_of(i, dy)
        p = place_of(i, dy)
        return rcopy(
            s_buf.at[pl.ds(m8(e * MSG), MSG), :],
            r_buf.at[pl.ds(p * MSG, MSG), :],
            pl_s.at[p], pl_r.at[p], (2 * e + k, x),
        )

    own_rows = pltpu.make_async_copy(
        s_buf.at[pl.ds(m8(c * MSG), MSG), :], r_buf.at[pl.ds(0, MSG), :], loc_sem.at[0]
    )
    own_rows.start()
    for i in range(NZ):
        for dy in range(NY):
            if i or dy:
                send_rows(i, dy).start()
    own_rows.wait()

    def col(off):
        return m8(((x + off) % NX) * Q, Q)

    def xa_at(core, g, off, kind=None):
        rows = pl.ds(m8(core * HALF + g * GROW, 16), GROW)
        if kind is None:
            return xa.at[:, rows, pl.ds(col(off), Q)]
        return xa.at[kind, rows, pl.ds(col(off), Q)]

    def x_copy(n, g):
        block, dev = (
            (xa_at(k, g, 0), right),
            (xa_at(k, g, 0), left),
            (xa_at(k, g, 0), mate),
            (xa_at(k, g, 3, 0), right),
            (xa_at(k, g, 1, 1), left),
            (xa_at(k, g, 3), mate),
            (xa_at(k, g, 1), mate),
            (xa_at(k, g, 2), mate),
        )[n]
        return rcopy(block, block, xs.at[n, g], xr.at[n, g], dev)

    def x_wait(n, g):
        block = (
            xa_at(k, g, 3),
            xa_at(k, g, 1),
            xa_at(1 - k, g, 0),
            xa_at(k, g, 2, 0),
            xa_at(k, g, 2, 1),
            xa_at(1 - k, g, 3),
            xa_at(1 - k, g, 1),
            xa_at(1 - k, g, 2),
        )[n]
        rcopy(block, block, xs.at[n, g], xr.at[n, g], mate).wait_recv()

    def plane_wait(buf, rows, sem_s, sem_r, p):
        block = buf.at[pl.ds(m8(p * rows), rows), :]
        rcopy(block, block, sem_s.at[p], sem_r.at[p], mate).wait_recv()

    def stage_in(g):
        def one(j, carry):
            p = g * 8 + j

            @pl.when(p > 0)
            def _():
                plane_wait(r_buf, MSG, pl_s, pl_r, p)

            return carry

        lax.fori_loop(0, 8, one, 0)
        got = nn(perm[...], r_buf[pl.ds(m8(g * 8 * MSG, 8 * MSG), 8 * MSG), :]).astype(BF16)
        rows = pl.ds(m8(k * HALF + g * GROW, 16), GROW)
        for kind in range(2):
            for part in range(2):
                n = 2 * kind + part
                xa[kind, rows, pl.ds(m8(qcol + part * 256, 256), 256)] = got[n * GROW : (n + 1) * GROW]
        for n in (0, 1, 2):
            x_copy(n, g).start()

    def stage_relay(g):
        x_wait(0, g)
        x_copy(3, g).start()
        x_copy(5, g).start()
        x_wait(1, g)
        x_copy(4, g).start()
        x_copy(6, g).start()

    def stage_far(g):
        x_wait(3, g)
        x_wait(4, g)
        x_copy(7, g).start()

    def both(buf, kind, g):
        return jnp.concatenate(
            [buf[kind, pl.ds(m8(core * HALF + g * GROW, 16), GROW), :] for core in range(2)], axis=0
        )

    def stage_compute(g):
        for n in (2, 5, 6, 7):
            x_wait(n, g)
        rows_n = both(xa, 0, g)
        pre_gate = nn(rows_n, wg[...])
        pre_up = nn(rows_n, wu[...])
        d_hidden = nt(both(xa, 1, g), wd[...])
        sig = jax.nn.sigmoid(pre_gate)
        act = pre_gate * sig
        hid_v = (act * pre_up).astype(BF16)
        dg_v = (d_hidden * pre_up * sig * (1.0 + pre_gate * (1.0 - sig))).astype(BF16)
        du_v = (d_hidden * act).astype(BF16)
        for core in range(2):
            rows = pl.ds(m8(core * HALF + g * GROW, 16), GROW)
            part = slice(core * GROW, (core + 1) * GROW)
            hid[rows, :] = hid_v[part]
            dga[rows, :] = dg_v[part]
            dup[rows, :] = du_v[part]

    def step(t, carry):
        @pl.when(t < GROUPS)
        def _():
            stage_in(t)

        @pl.when((t >= 1) & (t < GROUPS + 1))
        def _():
            stage_relay(t - 1)

        @pl.when((t >= 2) & (t < GROUPS + 2))
        def _():
            stage_far(t - 2)

        @pl.when(t == 3)
        def _():
            for copy in w_copies:
                copy.wait()

        @pl.when(t >= 3)
        def _():
            stage_compute(t - 3)

        return carry

    lax.fori_loop(0, GROUPS + 3, step, 0)

    def partial(o, core):
        rows = pl.ds(m8(core * HALF, 16), HALF)
        feats = pl.ds(col(O_OFF[o]), Q)
        return nt(dga[rows, :], wg[feats, :]) + nt(dup[rows, :], wu[feats, :])

    def mate_copy(o):
        return rcopy(ps.at[o], pr.at[o], q_s.at[o], q_r.at[o], mate)

    def make(o):
        ps[o] = partial(o, 1 - k).astype(BF16)
        mate_copy(o).start()
        po[o] = partial(o, k)

    half = HALF // 2
    e_copies = [
        rcopy(cs.at[0, pl.ds(0, half), :], ra, e_s.at[0], e_r.at[0], right),
        rcopy(cs.at[0, pl.ds(half, half), :], rb, e_s.at[1], e_r.at[1], left),
        rcopy(cs.at[1], rc, e_s.at[2], e_r.at[2], right),
        rcopy(cs.at[2], rd, e_s.at[3], e_r.at[3], left),
    ]
    make(0)
    make(1)
    mate_copy(0).wait_recv()
    cs[0] = (po[0] + pr[0].astype(F32)).astype(BF16)
    e_copies[0].start()
    e_copies[1].start()
    make(2)
    mate_copy(1).wait_recv()
    e_copies[0].wait_recv()
    total = po[1] + pr[1].astype(F32)
    cs[1, :half] = (total[:half] + ra[...].astype(F32)).astype(BF16)
    cs[1, half:] = total[half:].astype(BF16)
    e_copies[2].start()
    mate_copy(2).wait_recv()
    e_copies[1].wait_recv()
    total = po[2] + pr[2].astype(F32)
    cs[2, :half] = total[:half].astype(BF16)
    cs[2, half:] = (total[half:] + rb[...].astype(F32)).astype(BF16)
    e_copies[3].start()
    make(3)
    gdn_copy = pltpu.make_async_copy(gdn, gdn_o.at[0], out_sem.at[0])
    gup_copy = pltpu.make_async_copy(gup, gup_o.at[0], out_sem.at[1])

    def down_step(b, carry):
        cols = pl.ds(m8(b * 512, 512), 512)
        gdn[:, cols] = tn(hid[...], xa[1, :, cols]).astype(BF16)
        return carry

    def up_step(b, carry):
        cols = pl.ds(m8(b * 512, 512), 512)
        gup[cols, :] = tn(xa[0, :, cols], dup[...]).astype(BF16)
        return carry

    lax.fori_loop(0, 4, down_step, 0)
    gdn_copy.start()
    mate_copy(3).wait_recv()
    e_copies[2].wait_recv()
    e_copies[3].wait_recv()
    cs[3] = (po[3] + pr[3].astype(F32) + rc[...].astype(F32) + rd[...].astype(F32)).astype(BF16)

    def back_copy(p):
        src = source_of(p)
        return rcopy(
            rt.at[pl.ds(p * MSG, MSG), :],
            bk.at[pl.ds(m8(c * MSG), MSG), :],
            rt_s.at[p], rt_r.at[p], (2 * src + k, x),
        )

    for g in range(GROUPS):
        mine = cs[3, g * GROW : (g + 1) * GROW, :]
        stacked = jnp.concatenate([mine[:, j * 128 : (j + 1) * 128] for j in range(4)], axis=0)
        rt[g * 8 * MSG : (g + 1) * 8 * MSG, :] = nn(perm_t[...], stacked).astype(BF16)
        for j in range(8):
            p = g * 8 + j
            if p:
                back_copy(p).start()
    own_back = pltpu.make_async_copy(
        rt.at[pl.ds(0, MSG), :], bk.at[pl.ds(m8(c * MSG), MSG), :], loc_sem.at[1]
    )
    own_back.start()
    lax.fori_loop(0, 4, up_step, 0)
    gup_copy.start()
    own_back.wait()

    def back_wait(p, carry):
        block = bk.at[pl.ds(m8(p * MSG), MSG), :]
        rcopy(block, block, rt_s.at[p], rt_r.at[p], mate).wait_recv()
        return carry

    lax.fori_loop(1, CHIPS, back_wait, 0)

    cols = lax.broadcasted_iota(jnp.int32, (TOK, CHIPS * MSG), 1).astype(F32)
    back = bk[pl.ds(0, CHIPS * MSG), :]
    for j in range(4):
        hot = ((cols == s0 + j * CAP) | (cols == s1 + j * CAP)).astype(F32).astype(BF16)
        dn[:, pl.ds(m8(qcol + j * 128, 128), 128)] = nn(hot, back).astype(BF16)

    def dn_at(off, rows=None):
        return dn.at[pl.ds(0, TOK) if rows is None else pl.ds(rows, TOK // 2), pl.ds(col(off), Q)]

    def dn_copy(n):
        block, dev = (
            (dn_at(0), right), (dn_at(0), left), (dn_at(3, 0), right), (dn_at(1, TOK // 2), left)
        )[n]
        return rcopy(block, block, dn_s.at[n], dn_r.at[n], dev)

    def dn_wait(n):
        block = (dn_at(3), dn_at(1), dn_at(2, 0), dn_at(2, TOK // 2))[n]
        rcopy(block, block, dn_s.at[n], dn_r.at[n], mate).wait_recv()

    dn_copy(0).start()
    dn_copy(1).start()
    mixed = (ogate[...].astype(F32) * cout[...].astype(F32)).astype(BF16)
    dn_wait(0)
    dn_copy(2).start()
    dn_wait(1)
    dn_copy(3).start()
    dn_wait(2)
    dn_wait(3)

    d_norm = dn[...].astype(F32)
    unit = resid[...].astype(F32) * inv
    row_mean = jnp.mean(unit * d_norm, axis=-1, keepdims=True)
    gr = (og[...].astype(F32) + inv * (d_norm - unit * row_mean)).astype(BF16)
    gr_o[...] = gr

    grad_w = tn(gr, mixed).reshape(CHIPS, 2, 32, C)
    gacc[0] = grad_w[:, 0].reshape(CHIPS * 32, C)
    gacc[1] = grad_w[:, 1].reshape(CHIPS * 32, C)
    gb[...] = gacc[1 - k].astype(BF16)
    gmate = rcopy(gb, gp, t_s.at[0], t_r.at[0], mate)
    gmate.start()

    d_mix = nt(gr, wout[...])
    d_conv = d_mix * ogate[...].astype(F32)
    dcv[...] = d_conv
    to_after = rcopy(dcv.at[pl.ds(TOK - 8, 8), :], hp, t_s.at[1], t_r.at[1], after)
    to_before = rcopy(dcv.at[pl.ds(0, 8), :], hn, t_s.at[2], t_r.at[2], before)
    to_after.start()
    to_before.start()
    gog_o[...] = (d_mix * cout[...].astype(F32)).astype(BF16)

    gmate.wait_recv()
    gs[...] = (gacc[k] + gp[...].astype(F32)).astype(BF16)

    def g_copy(i, dy):
        e = expert_of(i, dy)
        p = place_of(i, dy)
        return rcopy(
            gs.at[pl.ds(m8(e * 32, 32), 32), :],
            g_in.at[pl.ds(p * 32, 32), :],
            g_s.at[p], g_r.at[p], (2 * e + k, x),
        )

    for i in range(NZ - 1, -1, -1):
        for dy in range(NY):
            if i or dy:
                g_copy(i, dy).start()
    own_g = pltpu.make_async_copy(
        gs.at[pl.ds(m8(c * 32, 32), 32), :], g_in.at[pl.ds(0, 32), :], loc_sem.at[2]
    )
    own_g.start()

    to_after.wait_recv()
    to_before.wait_recv()
    row = lax.broadcasted_iota(jnp.int32, (TOK, C), 0)
    next_row = jnp.where(s == 63, 0.0, hn[0:1, :])
    prev_row = jnp.where(s == 0, 0.0, hp[7:8, :])
    nxt = jnp.where(row == TOK - 1, next_row, pltpu.roll(d_conv, TOK - 1, 0))
    prv = jnp.where(row == 0, prev_row, pltpu.roll(d_conv, 1, 0))
    d_inner = taps[0:1, :] * nxt + taps[1:2, :] * d_conv + taps[2:3, :] * prv
    gig_o[...] = (d_inner * cin[...].astype(F32)).astype(BF16)
    gci_o[...] = (d_inner * igate[...].astype(F32)).astype(BF16)

    own_g.wait()

    def g_wait(p, carry):
        plane_wait(g_in, 32, g_s, g_r, p)
        return carry

    lax.fori_loop(1, CHIPS, g_wait, 0)
    gwo_o[...] = jnp.sum(g_in[...].reshape(CHIPS, 32, C).astype(F32), axis=0)

    for i in range(NZ):
        for dy in range(NY):
            if i or dy:
                send_rows(i, dy).wait_send()
                g_copy(i, dy).wait_send()
                back_copy(place_of(i, dy)).wait_send()

    def x_sent(g, carry):
        for n in range(8):
            x_copy(n, g).wait_send()
        return carry

    lax.fori_loop(0, GROUPS, x_sent, 0)
    for o in range(4):
        mate_copy(o).wait_send()
        e_copies[o].wait_send()
        dn_copy(o).wait_send()
    gmate.wait_send()
    to_after.wait_send()
    to_before.wait_send()
    gdn_copy.wait()
    gup_copy.wait()


def per_device(*args):
    place = permutation()
    perm = jnp.asarray(place, BF16)
    perm_t = jnp.asarray(place.T, BF16)
    vmem = pl.BlockSpec(memory_space=pltpu.VMEM)
    hbm = pl.BlockSpec(memory_space=pl.ANY)
    dma = pltpu.SemaphoreType.DMA
    in_specs = [vmem] * 4 + [hbm] * 3 + [vmem] * 8
    out_shape = [
        jax.ShapeDtypeStruct((TOK, D), BF16),
        jax.ShapeDtypeStruct((1, D, H), BF16),
        jax.ShapeDtypeStruct((1, H, D), BF16),
        jax.ShapeDtypeStruct((TOK, C), BF16),
        jax.ShapeDtypeStruct((TOK, C), BF16),
        jax.ShapeDtypeStruct((TOK, C), BF16),
        jax.ShapeDtypeStruct((32, C), F32),
    ]
    out_specs = [vmem, hbm, hbm, vmem, vmem, vmem, vmem]
    slots = CHIPS * MSG
    scratch = [
        pltpu.VMEM((D, H), BF16), pltpu.VMEM((D, H), BF16), pltpu.VMEM((H, D), BF16),
        pltpu.VMEM((slots + 8, 256), BF16), pltpu.VMEM((slots + 8, 256), BF16),
        pltpu.VMEM((2, 2 * HALF, D), BF16),
        pltpu.VMEM((2 * HALF, H), BF16), pltpu.VMEM((2 * HALF, H), BF16), pltpu.VMEM((2 * HALF, H), BF16),
        pltpu.VMEM((4, HALF, Q), BF16), pltpu.VMEM((4, HALF, Q), BF16), pltpu.VMEM((4, HALF, Q), F32),
        pltpu.VMEM((HALF // 2, Q), BF16), pltpu.VMEM((HALF // 2, Q), BF16),
        pltpu.VMEM((HALF, Q), BF16), pltpu.VMEM((HALF, Q), BF16), pltpu.VMEM((4, HALF, Q), BF16),
        pltpu.VMEM((slots + 8, 128), BF16), pltpu.VMEM((slots + 8, 128), BF16),
        pltpu.VMEM((TOK, D), BF16),
        pltpu.VMEM((2, 1024, C), F32), pltpu.VMEM((1024, C), BF16), pltpu.VMEM((1024, C), BF16),
        pltpu.VMEM((1024, C), BF16), pltpu.VMEM((1024, C), BF16),
        pltpu.VMEM((TOK, C), F32), pltpu.VMEM((8, C), F32), pltpu.VMEM((8, C), F32),
        pltpu.VMEM((D, H), BF16), pltpu.VMEM((H, D), BF16),
        dma((3,)), dma((3,)), dma((32,)), dma((32,)), dma((32,)), dma((32,)), dma((32,)), dma((32,)),
        dma((8, 4)), dma((8, 4)), dma((4,)), dma((4,)), dma((4,)), dma((4,)), dma((4,)), dma((4,)),
        dma((3,)), dma((3,)), dma((2,)),
    ]
    return pl.pallas_call(
        kernel,
        out_shape=out_shape,
        in_specs=in_specs,
        out_specs=out_specs,
        scratch_shapes=scratch,
        compiler_params=pltpu.CompilerParams(
            collective_id=0, has_side_effects=True, vmem_limit_bytes=60 * 1024 * 1024
        ),
    )(*args, perm, perm_t)


def solution(mesh):
    in_specs = (
        P("sp", None), P("sp", None), P("sp", None), P("sp", None),
        P("sp", None, "tp"), P("sp", None, "tp"), P("sp", "tp", None),
        P("sp", "tp"), P("sp", "tp"), P("sp", "tp"), P("sp", "tp"),
        P(None, "tp"), P("tp", None),
    )
    out_specs = (
        P("sp", None), P("sp", None, "tp"), P("sp", "tp", None),
        P("sp", "tp"), P("sp", "tp"), P("sp", "tp"), P("sp", "tp"),
    )
    return jax.shard_map(
        per_device, mesh=mesh, in_specs=in_specs, out_specs=out_specs, check_vma=False
    )
```

profile of v0, /device:TPU:1, one launch (start us, length us, event | category | flops | bytes accessed | tf_op | source)
XLA Modules:
  0.0 116.7 jit_solution(2344919551585135851)
XLA Ops:
  0.6 1.4 %copy.22.routes = s32[128,2]{1,0:T(8,128)} copy(s32[128,2]{0,1:T(2,128)} %param.17) | data formatting | bytes 2048 | tf_op args[2]
  2.0 1.4 %copy.23.rw = f32[128,2]{1,0:T(8,128)} copy(f32[128,2]{0,1:T(2,128)} %param.18) | data formatting | bytes 2048 | tf_op args[3]
  3.5 104.3 %shard_map.198 = (bf16[128,2048]{1,0:T(8,128)(2,1)}, bf16[1,2048,512]{2,1,0:T(8,128)(2,1)}, bf16[1,512,2048]{2,1,0:T(8,128)(2,1)}, bf16[128,256]{1,0:T(8,128)(2,...) custom-call(bf16[128,2048]{1,0:T(8,128)(2,1)} %og.1, bf16[128,2048]{1,0:T(8,128)(2,1)} %resid.1, ...), custom_call_target="tpu_custom_call" | custom-call | tf_op jit(solution)/shard_map/pallas_call | solution.py:543
  107.8 1.9 %copy.31 = bf16[128,2048]{1,0:T(8,128)(2,1)} copy(bf16[128,2048]{1,0:T(8,128)(2,1)} %get-tuple-element.14) | data formatting | bytes 1048576
  109.7 0.0 copy-start
  109.7 3.2 %copy.32 = bf16[1,2048,512]{2,1,0:T(8,128)(2,1)} copy(bf16[1,2048,512]{2,1,0:T(8,128)(2,1)} %get-tuple-element.15) | data formatting | bytes 4194304
  112.9 0.0 copy-done
  112.9 0.0 copy-start.3
  112.9 0.0 copy-start.2
  112.9 0.0 copy-start.1
  112.9 0.0 copy-start.4
  112.9 1.3 %copy.33 = bf16[1,512,2048]{2,1,0:T(8,128)(2,1)} copy(bf16[1,512,2048]{2,1,0:T(8,128)(2,1)S(1)} %copy-done) | data formatting | bytes 4194304
  114.2 0.0 copy-done.3
  114.2 0.6 copy.34
  114.8 0.0 copy-done.2
  114.8 0.6 copy.35
  115.5 0.0 copy-done.1
  115.5 0.6 copy.36
  116.1 0.0 copy-done.4
  116.1 0.6 copy.37
Async XLA Ops:
  109.7 3.2 %copy-start = (bf16[1,512,2048]{2,1,0:T(8,128)(2,1)S(1)}, bf16[1,512,2048]{2,1,0:T(8,128)(2,1)}, u32[]{:S(2)}) copy-start(bf16[1,512,2048]{2,1,0:T(8,128)(2,1)} %get-tuple-element.16) | copy-start | bytes 6291460
  112.9 1.3 %copy-start.3 = (bf16[128,256]{1,0:T(8,128)(2,1)S(1)}, bf16[128,256]{1,0:T(8,128)(2,1)}, u32[]{:S(2)}) copy-start(bf16[128,256]{1,0:T(8,128)(2,1)} %get-tuple-element.17) | copy-start | bytes 196612
  112.9 2.0 %copy-start.2 = (bf16[128,256]{1,0:T(8,128)(2,1)S(1)}, bf16[128,256]{1,0:T(8,128)(2,1)}, u32[]{:S(2)}) copy-start(bf16[128,256]{1,0:T(8,128)(2,1)} %get-tuple-element.18) | copy-start | bytes 196612
  112.9 2.6 %copy-start.1 = (bf16[128,256]{1,0:T(8,128)(2,1)S(1)}, bf16[128,256]{1,0:T(8,128)(2,1)}, u32[]{:S(2)}) copy-start(bf16[128,256]{1,0:T(8,128)(2,1)} %get-tuple-element.19) | copy-start | bytes 196612
  112.9 3.2 %copy-start.4 = (f32[32,256]{1,0:T(8,128)S(1)}, f32[32,256]{1,0:T(8,128)}, u32[]{:S(2)}) copy-start(f32[32,256]{1,0:T(8,128)} %get-tuple-element.20) | copy-start | bytes 98308
where the time goes:
time: 118 us; the launch traced here: 117 us
  Pallas kernels  104 us (88%)
  local copies, waits for them, and re-layouts  11.7 us (10%)
    pallas_call x1, Pallas kernels, per_device(): pl.pallas_call(kernel, out_shape=out_shape, in_specs=in_specs, out_specs=...  104 us
    unnamed x19, local copies, waits for them, and re-layouts  11.7 us

commit v1 on v0

--- a/solution.py
+++ b/solution.py
@@ -53,11 +53,13 @@
 
 
 def kernel(
-    og, resid, routes, rw, wg_h, wu_h, wd_h, ogate, igate, cin, cout, taps, wout, perm, perm_t,
+    og_h, resid_h, routes_h, rw_h, wg_h, wu_h, wd_h, ogate_h, igate_h, cin_h, cout_h, taps_h, wout_h,
+    perm_h, perm_t_h,
     gr_o, gup_o, gdn_o, gog_o, gig_o, gci_o, gwo_o,
+    og, resid, routes, rw, ogate, igate, cin, cout, taps, wout, perm, perm_t,
     wg, wu, wd, s_buf, r_buf, xa, hid, dga, dup, ps, pr, po, ra, rb, rc, rd, cs, rt, bk, dn,
-    gacc, gb, gp, gs, g_in, dcv, hp, hn, gup, gdn,
-    w_sem, loc_sem, pl_s, pl_r, rt_s, rt_r, g_s, g_r, xs, xr, q_s, q_r, e_s, e_r, dn_s, dn_r, t_s, t_r, out_sem,
+    gacc, gb, gp, gs, g_in, dcv, hp, hn,
+    w_sem, loc_sem, pl_s, pl_r, rt_s, rt_r, g_s, g_r, xs, xr, q_s, q_r, e_s, e_r, dn_s, dn_r, t_s, t_r,
 ):
     s = lax.axis_index("sp")
     x = lax.axis_index("tp")
@@ -75,9 +77,6 @@
     def expert_of(i, dy):
         return ((z + NZ - Z_ORDER[i]) % NZ) * NY + (y + dy) % NY
 
-    def source_of(p):
-        return ((z + Z_ORDER[p // NY]) % NZ) * NY + (y + p % NY) % NY
-
     def place_of(i, dy):
         return i * NY + (NY - dy) % NY
 
@@ -96,35 +95,51 @@
     for dev in (right, left, mate, across):
         pl.semaphore_signal(barrier, inc=1, device_id=dev, device_id_type=MESH)
 
-    w_copies = [
-        pltpu.make_async_copy(wg_h.at[0], wg, w_sem.at[0]),
-        pltpu.make_async_copy(wu_h.at[0], wu, w_sem.at[1]),
-        pltpu.make_async_copy(wd_h.at[0], wd, w_sem.at[2]),
+    loads = [
+        pltpu.make_async_copy(src, dst, w_sem.at[n])
+        for n, (src, dst) in enumerate(
+            (
+                (routes_h, routes), (rw_h, rw), (resid_h, resid), (og_h, og), (perm_h, perm),
+                (wg_h.at[0], wg), (wu_h.at[0], wu), (wd_h.at[0], wd),
+                (perm_t_h, perm_t), (ogate_h, ogate), (cout_h, cout), (wout_h, wout),
+                (cin_h, cin), (igate_h, igate), (taps_h, taps),
+            )
+        )
     ]
-    for copy in w_copies:
+    for copy in loads[:5]:
         copy.start()
 
+    loads[0].wait()
+    loads[1].wait()
     lanes = lax.broadcasted_iota(jnp.int32, (TOK, TOK), 1)
     subs = lax.broadcasted_iota(jnp.int32, (TOK, TOK), 0)
-    r0 = routes[:, 0:1]
-    r1 = routes[:, 1:2]
-    a0 = (lanes == r0).astype(F32)
-    a1 = (lanes == r1).astype(F32)
+    eye = lanes == subs
+
+    def column(row):
+        return jnp.sum(jnp.where(eye, row.astype(F32), 0.0), axis=1, keepdims=True)
+
+    r0 = column(routes[0:1, :])
+    r1 = column(routes[1:2, :])
+    w0 = column(rw[0:1, :])
+    w1 = column(rw[1:2, :])
+    a0 = (lanes.astype(F32) == r0).astype(F32)
+    a1 = (lanes.astype(F32) == r1).astype(F32)
     earlier = (lanes < subs).astype(F32).astype(BF16)
     counts = nn(earlier, (a0 + a1).astype(BF16))
-    s0 = r0.astype(F32) * MSG + jnp.sum(a0 * counts, axis=1, keepdims=True)
-    s1 = r1.astype(F32) * MSG + jnp.sum(a1 * counts, axis=1, keepdims=True)
-    eye = lanes == subs
+    s0 = r0 * MSG + jnp.sum(a0 * counts, axis=1, keepdims=True)
+    s1 = r1 * MSG + jnp.sum(a1 * counts, axis=1, keepdims=True)
     s0_row = jnp.sum(jnp.where(eye, s0, 0.0), axis=0, keepdims=True)
     s1_row = jnp.sum(jnp.where(eye, s1, 0.0), axis=0, keepdims=True)
 
+    loads[2].wait()
+    loads[3].wait()
     rf = resid[...].astype(F32)
     inv = lax.rsqrt(jnp.mean(rf * rf, axis=-1, keepdims=True) + EPS)
     qcol = m8(x * Q, Q)
     norm_q = (resid[:, pl.ds(qcol, Q)].astype(F32) * inv).astype(BF16)
     og_q = og[:, pl.ds(qcol, Q)].astype(F32)
-    w0_q = (rw[:, 0:1] * og_q).astype(BF16)
-    w1_q = (rw[:, 1:2] * og_q).astype(BF16)
+    w0_q = (w0 * og_q).astype(BF16)
+    w1_q = (w1 * og_q).astype(BF16)
     data = jnp.concatenate(
         [
             norm_q[:, :256], norm_q[:, 256:],
@@ -151,7 +166,10 @@
         s_buf[pl.ds(m8(b * 8 * MSG, 8 * MSG), 8 * MSG), :] = nn(picks, data).astype(BF16)
         return carry
 
+    for copy in loads[5:]:
+        copy.start()
     lax.fori_loop(0, GROUPS, build, 0)
+    loads[4].wait()
 
     pl.semaphore_wait(barrier, 35)
 
@@ -270,6 +288,84 @@
             dga[rows, :] = dg_v[part]
             dup[rows, :] = du_v[part]
 
+    def mate_copy(g):
+        return rcopy(ps.at[g], pr.at[g], q_s.at[g], q_r.at[g], mate)
+
+    def e_copy(n, g):
+        src, dst, dev = (
+            (cs.at[g, 0, :, pl.ds(0, 256)], ra.at[g], right),
+            (cs.at[g, 0, :, pl.ds(256, 256)], rb.at[g], left),
+            (cs.at[g, 1], rc.at[g], right),
+            (cs.at[g, 2], rd.at[g], left),
+        )[n]
+        return rcopy(src, dst, e_s.at[n, g], e_r.at[n, g], dev)
+
+    def back_copy(p, source):
+        return rcopy(
+            rt.at[pl.ds(m8(p * MSG), MSG), :],
+            bk.at[pl.ds(m8(c * MSG), MSG), :],
+            rt_s.at[p], rt_r.at[p], (2 * source + k, x),
+        )
+
+    def source_in(g, j):
+        away = (NZ - g) % NZ if j < NY else g + 1
+        return ((z + away) % NZ) * NY + (y + j % NY) % NY
+
+    def stage_make(g):
+        d_gate = jnp.concatenate(
+            [dga[pl.ds(m8(core * HALF + g * GROW, 16), GROW), :] for core in (1 - k, k)], axis=0
+        )
+        d_up = jnp.concatenate(
+            [dup[pl.ds(m8(core * HALF + g * GROW, 16), GROW), :] for core in (1 - k, k)], axis=0
+        )
+        for o in range(4):
+            feats = pl.ds(col(O_OFF[o]), Q)
+            part = nt(d_gate, wg[feats, :]) + nt(d_up, wu[feats, :])
+            ps[g, o] = part[:GROW].astype(BF16)
+            po[g, o] = part[GROW:]
+        mate_copy(g).start()
+
+    def stage_first(g):
+        mate_copy(g).wait_recv()
+        cs[g, 0] = (po[g, 0] + pr[g, 0].astype(F32)).astype(BF16)
+        e_copy(0, g).start()
+        e_copy(1, g).start()
+
+    def stage_second(g):
+        total = po[g, 1] + pr[g, 1].astype(F32)
+        e_copy(0, g).wait_recv()
+        cs[g, 1, :, 0:256] = (total[:, :256] + ra[g].astype(F32)).astype(BF16)
+        cs[g, 1, :, 256:512] = total[:, 256:].astype(BF16)
+        e_copy(2, g).start()
+        total = po[g, 2] + pr[g, 2].astype(F32)
+        e_copy(1, g).wait_recv()
+        cs[g, 2, :, 0:256] = total[:, :256].astype(BF16)
+        cs[g, 2, :, 256:512] = (total[:, 256:] + rb[g].astype(F32)).astype(BF16)
+        e_copy(3, g).start()
+
+    def stage_back(g):
+        e_copy(2, g).wait_recv()
+        e_copy(3, g).wait_recv()
+        mine = (po[g, 3] + pr[g, 3].astype(F32) + rc[g].astype(F32) + rd[g].astype(F32)).astype(BF16)
+        stacked = jnp.concatenate([mine[:, j * 128 : (j + 1) * 128] for j in range(4)], axis=0)
+        rt[pl.ds(m8(g * 8 * MSG, 8 * MSG), 8 * MSG), :] = nn(perm_t[...], stacked).astype(BF16)
+        for j in range(8):
+            copy = back_copy(g * 8 + j, source_in(g, j))
+            if j:
+                copy.start()
+            else:
+                pl.when(g > 0)(copy.start)
+
+    def down_step(b, carry):
+        cols = pl.ds(m8(b * 512, 512), 512)
+        gdn_o[0, :, cols] = tn(hid[...], xa[1, :, cols]).astype(BF16)
+        return carry
+
+    def up_step(b, carry):
+        cols = pl.ds(m8(b * 512, 512), 512)
+        gup_o[0, cols, :] = tn(xa[0, :, cols], dup[...]).astype(BF16)
+        return carry
+
     def step(t, carry):
         @pl.when(t < GROUPS)
         def _():
@@ -285,99 +381,39 @@
 
         @pl.when(t == 3)
         def _():
-            for copy in w_copies:
+            for copy in loads[5:]:
                 copy.wait()
 
-        @pl.when(t >= 3)
+        @pl.when((t >= 3) & (t < GROUPS + 3))
         def _():
             stage_compute(t - 3)
+            stage_make(t - 3)
+
+        @pl.when((t >= 4) & (t < GROUPS + 4))
+        def _():
+            stage_first(t - 4)
+
+        @pl.when(t == GROUPS + 4)
+        def _():
+            lax.fori_loop(0, 4, down_step, 0)
+
+        @pl.when((t >= 5) & (t < GROUPS + 5))
+        def _():
+            stage_second(t - 5)
+
+        @pl.when(t >= 6)
+        def _():
+            stage_back(t - 6)
 
         return carry
 
-    lax.fori_loop(0, GROUPS + 3, step, 0)
-
-    def partial(o, core):
-        rows = pl.ds(m8(core * HALF, 16), HALF)
-        feats = pl.ds(col(O_OFF[o]), Q)
-        return nt(dga[rows, :], wg[feats, :]) + nt(dup[rows, :], wu[feats, :])
-
-    def mate_copy(o):
-        return rcopy(ps.at[o], pr.at[o], q_s.at[o], q_r.at[o], mate)
-
-    def make(o):
-        ps[o] = partial(o, 1 - k).astype(BF16)
-        mate_copy(o).start()
-        po[o] = partial(o, k)
-
-    half = HALF // 2
-    e_copies = [
-        rcopy(cs.at[0, pl.ds(0, half), :], ra, e_s.at[0], e_r.at[0], right),
-        rcopy(cs.at[0, pl.ds(half, half), :], rb, e_s.at[1], e_r.at[1], left),
-        rcopy(cs.at[1], rc, e_s.at[2], e_r.at[2], right),
-        rcopy(cs.at[2], rd, e_s.at[3], e_r.at[3], left),
-    ]
-    make(0)
-    make(1)
-    mate_copy(0).wait_recv()
-    cs[0] = (po[0] + pr[0].astype(F32)).astype(BF16)
-    e_copies[0].start()
-    e_copies[1].start()
-    make(2)
-    mate_copy(1).wait_recv()
-    e_copies[0].wait_recv()
-    total = po[1] + pr[1].astype(F32)
-    cs[1, :half] = (total[:half] + ra[...].astype(F32)).astype(BF16)
-    cs[1, half:] = total[half:].astype(BF16)
-    e_copies[2].start()
-    mate_copy(2).wait_recv()
-    e_copies[1].wait_recv()
-    total = po[2] + pr[2].astype(F32)
-    cs[2, :half] = total[:half].astype(BF16)
-    cs[2, half:] = (total[half:] + rb[...].astype(F32)).astype(BF16)
-    e_copies[3].start()
-    make(3)
-    gdn_copy = pltpu.make_async_copy(gdn, gdn_o.at[0], out_sem.at[0])
-    gup_copy = pltpu.make_async_copy(gup, gup_o.at[0], out_sem.at[1])
-
-    def down_step(b, carry):
-        cols = pl.ds(m8(b * 512, 512), 512)
-        gdn[:, cols] = tn(hid[...], xa[1, :, cols]).astype(BF16)
-        return carry
-
-    def up_step(b, carry):
-        cols = pl.ds(m8(b * 512, 512), 512)
-        gup[cols, :] = tn(xa[0, :, cols], dup[...]).astype(BF16)
-        return carry
-
-    lax.fori_loop(0, 4, down_step, 0)
-    gdn_copy.start()
-    mate_copy(3).wait_recv()
-    e_copies[2].wait_recv()
-    e_copies[3].wait_recv()
-    cs[3] = (po[3] + pr[3].astype(F32) + rc[...].astype(F32) + rd[...].astype(F32)).astype(BF16)
-
-    def back_copy(p):
-        src = source_of(p)
-        return rcopy(
-            rt.at[pl.ds(p * MSG, MSG), :],
-            bk.at[pl.ds(m8(c * MSG), MSG), :],
-            rt_s.at[p], rt_r.at[p], (2 * src + k, x),
-        )
-
-    for g in range(GROUPS):
-        mine = cs[3, g * GROW : (g + 1) * GROW, :]
-        stacked = jnp.concatenate([mine[:, j * 128 : (j + 1) * 128] for j in range(4)], axis=0)
-        rt[g * 8 * MSG : (g + 1) * 8 * MSG, :] = nn(perm_t[...], stacked).astype(BF16)
-        for j in range(8):
-            p = g * 8 + j
-            if p:
-                back_copy(p).start()
+    lax.fori_loop(0, GROUPS + 6, step, 0)
+
     own_back = pltpu.make_async_copy(
         rt.at[pl.ds(0, MSG), :], bk.at[pl.ds(m8(c * MSG), MSG), :], loc_sem.at[1]
     )
     own_back.start()
     lax.fori_loop(0, 4, up_step, 0)
-    gup_copy.start()
     own_back.wait()
 
     def back_wait(p, carry):
@@ -484,23 +520,36 @@
             if i or dy:
                 send_rows(i, dy).wait_send()
                 g_copy(i, dy).wait_send()
-                back_copy(place_of(i, dy)).wait_send()
 
     def x_sent(g, carry):
         for n in range(8):
             x_copy(n, g).wait_send()
+        mate_copy(g).wait_send()
+        for n in range(4):
+            e_copy(n, g).wait_send()
+        for j in range(8):
+            copy = back_copy(g * 8 + j, source_in(g, j))
+            if j:
+                copy.wait_send()
+            else:
+                pl.when(g > 0)(copy.wait_send)
         return carry
 
     lax.fori_loop(0, GROUPS, x_sent, 0)
-    for o in range(4):
-        mate_copy(o).wait_send()
-        e_copies[o].wait_send()
-        dn_copy(o).wait_send()
+    for n in range(4):
+        dn_copy(n).wait_send()
     gmate.wait_send()
     to_after.wait_send()
     to_before.wait_send()
-    gdn_copy.wait()
-    gup_copy.wait()
+
+
+def finish(*refs):
+    ins, outs, sems = refs[:7], refs[7:14], refs[14]
+    copies = [pltpu.make_async_copy(a, b, sems.at[n]) for n, (a, b) in enumerate(zip(ins, outs))]
+    for copy in copies:
+        copy.start()
+    for copy in copies:
+        copy.wait()
 
 
 def per_device(*args):
@@ -510,46 +559,53 @@
     vmem = pl.BlockSpec(memory_space=pltpu.VMEM)
     hbm = pl.BlockSpec(memory_space=pl.ANY)
     dma = pltpu.SemaphoreType.DMA
-    in_specs = [vmem] * 4 + [hbm] * 3 + [vmem] * 8
-    out_shape = [
-        jax.ShapeDtypeStruct((TOK, D), BF16),
-        jax.ShapeDtypeStruct((1, D, H), BF16),
-        jax.ShapeDtypeStruct((1, H, D), BF16),
-        jax.ShapeDtypeStruct((TOK, C), BF16),
-        jax.ShapeDtypeStruct((TOK, C), BF16),
-        jax.ShapeDtypeStruct((TOK, C), BF16),
-        jax.ShapeDtypeStruct((32, C), F32),
+    shapes = [
+        ((TOK, D), BF16), ((1, D, H), BF16), ((1, H, D), BF16),
+        ((TOK, C), BF16), ((TOK, C), BF16), ((TOK, C), BF16), ((32, C), F32),
     ]
-    out_specs = [vmem, hbm, hbm, vmem, vmem, vmem, vmem]
     slots = CHIPS * MSG
     scratch = [
+        pltpu.VMEM((TOK, D), BF16), pltpu.VMEM((TOK, D), BF16),
+        pltpu.VMEM((2, TOK), jnp.int32), pltpu.VMEM((2, TOK), F32),
+        pltpu.VMEM((TOK, C), BF16), pltpu.VMEM((TOK, C), BF16), pltpu.VMEM((TOK, C), BF16), pltpu.VMEM((TOK, C), BF16),
+        pltpu.VMEM((3, C), F32), pltpu.VMEM((C, D), BF16),
+        pltpu.VMEM((8 * MSG, 8 * MSG), BF16), pltpu.VMEM((8 * MSG, 8 * MSG), BF16),
         pltpu.VMEM((D, H), BF16), pltpu.VMEM((D, H), BF16), pltpu.VMEM((H, D), BF16),
         pltpu.VMEM((slots + 8, 256), BF16), pltpu.VMEM((slots + 8, 256), BF16),
         pltpu.VMEM((2, 2 * HALF, D), BF16),
         pltpu.VMEM((2 * HALF, H), BF16), pltpu.VMEM((2 * HALF, H), BF16), pltpu.VMEM((2 * HALF, H), BF16),
-        pltpu.VMEM((4, HALF, Q), BF16), pltpu.VMEM((4, HALF, Q), BF16), pltpu.VMEM((4, HALF, Q), F32),
-        pltpu.VMEM((HALF // 2, Q), BF16), pltpu.VMEM((HALF // 2, Q), BF16),
-        pltpu.VMEM((HALF, Q), BF16), pltpu.VMEM((HALF, Q), BF16), pltpu.VMEM((4, HALF, Q), BF16),
+        pltpu.VMEM((GROUPS, 4, GROW, Q), BF16), pltpu.VMEM((GROUPS, 4, GROW, Q), BF16),
+        pltpu.VMEM((GROUPS, 4, GROW, Q), F32),
+        pltpu.VMEM((GROUPS, GROW, 256), BF16), pltpu.VMEM((GROUPS, GROW, 256), BF16),
+        pltpu.VMEM((GROUPS, GROW, Q), BF16), pltpu.VMEM((GROUPS, GROW, Q), BF16),
+        pltpu.VMEM((GROUPS, 4, GROW, Q), BF16),
         pltpu.VMEM((slots + 8, 128), BF16), pltpu.VMEM((slots + 8, 128), BF16),
         pltpu.VMEM((TOK, D), BF16),
         pltpu.VMEM((2, 1024, C), F32), pltpu.VMEM((1024, C), BF16), pltpu.VMEM((1024, C), BF16),
         pltpu.VMEM((1024, C), BF16), pltpu.VMEM((1024, C), BF16),
         pltpu.VMEM((TOK, C), F32), pltpu.VMEM((8, C), F32), pltpu.VMEM((8, C), F32),
-        pltpu.VMEM((D, H), BF16), pltpu.VMEM((H, D), BF16),
-        dma((3,)), dma((3,)), dma((32,)), dma((32,)), dma((32,)), dma((32,)), dma((32,)), dma((32,)),
-        dma((8, 4)), dma((8, 4)), dma((4,)), dma((4,)), dma((4,)), dma((4,)), dma((4,)), dma((4,)),
-        dma((3,)), dma((3,)), dma((2,)),
+        dma((15,)), dma((3,)), dma((32,)), dma((32,)), dma((32,)), dma((32,)), dma((32,)), dma((32,)),
+        dma((8, 4)), dma((8, 4)), dma((4,)), dma((4,)), dma((4, 4)), dma((4, 4)), dma((4,)), dma((4,)),
+        dma((3,)), dma((3,)),
     ]
-    return pl.pallas_call(
+    made = pl.pallas_call(
         kernel,
-        out_shape=out_shape,
-        in_specs=in_specs,
-        out_specs=out_specs,
+        out_shape=[pltpu.VMEM(*shape) for shape in shapes],
+        in_specs=[hbm] * 15,
+        out_specs=[vmem] * 7,
         scratch_shapes=scratch,
         compiler_params=pltpu.CompilerParams(
-            collective_id=0, has_side_effects=True, vmem_limit_bytes=60 * 1024 * 1024
+            collective_id=0, has_side_effects=True, vmem_limit_bytes=56 * 1024 * 1024
         ),
-    )(*args, perm, perm_t)
+    )(*args[:2], args[2].T, args[3].T, *args[4:], perm, perm_t)
+    return pl.pallas_call(
+        finish,
+        out_shape=[jax.ShapeDtypeStruct(*shape) for shape in shapes],
+        in_specs=[vmem] * 7,
+        out_specs=[hbm] * 7,
+        scratch_shapes=[dma((7,))],
+        compiler_params=pltpu.CompilerParams(vmem_limit_bytes=1024 * 1024),
+    )(*made)
 
 
 def solution(mesh):

time: 118 us -> 101 us (0.86); the launches traced: 117 us -> 101 us
  local copies, waits for them, and re-layouts: 11.7 us -> 0 us
  Pallas kernels: 104 us -> 100 us
    unnamed x19 -> x0, local copies, waits for them, and re-layouts: 11.7 us -> none
    pallas_call x1 -> x2, Pallas kernels: 104 us -> 100 us  [the longest x1 98.1 us: per_device(): pl.pallas_call(kernel, out_shape=[pltpu.VMEM(*shape) for shape in shapes]...]
where the time goes in v1:
time: 101 us
  Pallas kernels  100 us (99%)
    pallas_call x1, Pallas kernels, per_device(): pl.pallas_call(kernel, out_shape=[pltpu.VMEM(*shape) for shape in shapes]...  98.1 us
    pallas_call x1, Pallas kernels, per_device(): pl.pallas_call(finish, out_shape=[jax.ShapeDtypeStruct(*shape) for shape...  2.29 us

profile of v1, /device:TPU:1, one launch (start us, length us, event | category | flops | bytes accessed | tf_op | source)
XLA Modules:
  0.0 101.0 jit_solution(6296861455152390566)
XLA Ops:
  0.6 98.1 %shard_map.198 = (bf16[128,2048]{1,0:T(8,128)(2,1)S(1)}, bf16[1,2048,512]{2,1,0:T(8,128)(2,1)S(1)}, bf16[1,512,2048]{2,1,0:T(8,128)(2,1)S(1)}, bf16[128,256]{1,0...) custom-call(bf16[128,2048]{1,0:T(8,128)(2,1)} %og_h.1, ...), custom_call_target="tpu_custom_call" | custom-call | tf_op jit(solution)/shard_map/pallas_call | solution.py:591
  98.7 2.3 %shard_map.199 = (bf16[128,2048]{1,0:T(8,128)(2,1)}, bf16[1,2048,512]{2,1,0:T(8,128)(2,1)}, bf16[1,512,2048]{2,1,0:T(8,128)(2,1)}, bf16[128,256]{1,0:T(8,128)(2,...) custom-call(bf16[128,2048]{1,0:T(8,128)(2,1)S(1)} %get-tuple-element.14.refs_0_, ...), custom_call_target="tpu_custom_call" | custom-call | tf_op jit(solution)/shard_map/pallas_call | solution.py:601

commit v2 on v1

--- a/solution.py
+++ b/solution.py
@@ -24,6 +24,7 @@
 HALF = GROUPS * GROW
 C = 256
 Z_ORDER = (0, 1, 7, 2, 6, 3, 5, 4)
+W_ORDER = (4, 3, 5, 2, 6, 1, 7, 0)
 O_OFF = (2, 1, 3, 0)
 
 
@@ -58,8 +59,8 @@
     gr_o, gup_o, gdn_o, gog_o, gig_o, gci_o, gwo_o,
     og, resid, routes, rw, ogate, igate, cin, cout, taps, wout, perm, perm_t,
     wg, wu, wd, s_buf, r_buf, xa, hid, dga, dup, ps, pr, po, ra, rb, rc, rd, cs, rt, bk, dn,
-    gacc, gb, gp, gs, g_in, dcv, hp, hn,
-    w_sem, loc_sem, pl_s, pl_r, rt_s, rt_r, g_s, g_r, xs, xr, q_s, q_r, e_s, e_r, dn_s, dn_r, t_s, t_r,
+    gacc, gb, gp, gs, gy_in, gz_out, gz_in, dcv, halo,
+    w_sem, loc_sem, send_sem, pl_r, xr, q_r, e_r, dn_r, g_r, one_r,
 ):
     s = lax.axis_index("sp")
     x = lax.axis_index("tp")
@@ -179,7 +180,7 @@
         return rcopy(
             s_buf.at[pl.ds(m8(e * MSG), MSG), :],
             r_buf.at[pl.ds(p * MSG, MSG), :],
-            pl_s.at[p], pl_r.at[p], (2 * e + k, x),
+            send_sem.at[0], pl_r.at[i // 2], (2 * e + k, x),
         )
 
     own_rows = pltpu.make_async_copy(
@@ -212,36 +213,32 @@
             (xa_at(k, g, 1), mate),
             (xa_at(k, g, 2), mate),
         )[n]
-        return rcopy(block, block, xs.at[n, g], xr.at[n, g], dev)
+        return rcopy(block, block, send_sem.at[1], xr.at[(0, 1, 3, 2, 2, 3, 3, 3)[n], g], dev)
 
     def x_wait(n, g):
         block = (
-            xa_at(k, g, 3),
-            xa_at(k, g, 1),
-            xa_at(1 - k, g, 0),
-            xa_at(k, g, 2, 0),
-            xa_at(k, g, 2, 1),
-            xa_at(1 - k, g, 3),
-            xa_at(1 - k, g, 1),
-            xa_at(1 - k, g, 2),
-        )[n]
-        rcopy(block, block, xs.at[n, g], xr.at[n, g], mate).wait_recv()
-
-    def plane_wait(buf, rows, sem_s, sem_r, p):
-        block = buf.at[pl.ds(m8(p * rows), rows), :]
-        rcopy(block, block, sem_s.at[p], sem_r.at[p], mate).wait_recv()
+            lambda: xa_at(k, g, 3),
+            lambda: xa_at(k, g, 1),
+            lambda: xa_at(k, g, 2),
+            lambda: xa.at[:, pl.ds(m8((1 - k) * HALF + g * GROW, 16), GROW), :],
+        )[n]()
+        rcopy(block, block, send_sem.at[1], xr.at[n, g], mate).wait_recv()
+
+    def take(block, sem):
+        rcopy(block, block, sem, sem, mate).wait_recv()
+
+    def sent(block, sem):
+        rcopy(block, block, sem, sem, mate).wait_send()
 
     def stage_in(g):
-        def one(j, carry):
-            p = g * 8 + j
-
-            @pl.when(p > 0)
-            def _():
-                plane_wait(r_buf, MSG, pl_s, pl_r, p)
-
-            return carry
-
-        lax.fori_loop(0, 8, one, 0)
+        @pl.when(g == 0)
+        def _():
+            take(r_buf.at[pl.ds(MSG, 7 * MSG), :], pl_r.at[0])
+
+        @pl.when(g > 0)
+        def _():
+            take(r_buf.at[pl.ds(m8(g * 8 * MSG, 8 * MSG), 8 * MSG), :], pl_r.at[g])
+
         got = nn(perm[...], r_buf[pl.ds(m8(g * 8 * MSG, 8 * MSG), 8 * MSG), :]).astype(BF16)
         rows = pl.ds(m8(k * HALF + g * GROW, 16), GROW)
         for kind in range(2):
@@ -260,8 +257,7 @@
         x_copy(6, g).start()
 
     def stage_far(g):
-        x_wait(3, g)
-        x_wait(4, g)
+        x_wait(2, g)
         x_copy(7, g).start()
 
     def both(buf, kind, g):
@@ -270,8 +266,7 @@
         )
 
     def stage_compute(g):
-        for n in (2, 5, 6, 7):
-            x_wait(n, g)
+        x_wait(3, g)
         rows_n = both(xa, 0, g)
         pre_gate = nn(rows_n, wg[...])
         pre_up = nn(rows_n, wu[...])
@@ -289,7 +284,7 @@
             dup[rows, :] = du_v[part]
 
     def mate_copy(g):
-        return rcopy(ps.at[g], pr.at[g], q_s.at[g], q_r.at[g], mate)
+        return rcopy(ps.at[g], pr.at[g], send_sem.at[2], q_r.at[g], mate)
 
     def e_copy(n, g):
         src, dst, dev = (
@@ -298,13 +293,13 @@
             (cs.at[g, 1], rc.at[g], right),
             (cs.at[g, 2], rd.at[g], left),
         )[n]
-        return rcopy(src, dst, e_s.at[n, g], e_r.at[n, g], dev)
+        return rcopy(src, dst, send_sem.at[3], e_r.at[n // 2, g], dev)
 
     def back_copy(p, source):
         return rcopy(
             rt.at[pl.ds(m8(p * MSG), MSG), :],
             bk.at[pl.ds(m8(c * MSG), MSG), :],
-            rt_s.at[p], rt_r.at[p], (2 * source + k, x),
+            send_sem.at[4], one_r.at[0], (2 * source + k, x),
         )
 
     def source_in(g, j):
@@ -332,20 +327,18 @@
         e_copy(1, g).start()
 
     def stage_second(g):
+        take(cs.at[g, 0], e_r.at[0, g])
         total = po[g, 1] + pr[g, 1].astype(F32)
-        e_copy(0, g).wait_recv()
         cs[g, 1, :, 0:256] = (total[:, :256] + ra[g].astype(F32)).astype(BF16)
         cs[g, 1, :, 256:512] = total[:, 256:].astype(BF16)
         e_copy(2, g).start()
         total = po[g, 2] + pr[g, 2].astype(F32)
-        e_copy(1, g).wait_recv()
         cs[g, 2, :, 0:256] = total[:, :256].astype(BF16)
         cs[g, 2, :, 256:512] = (total[:, 256:] + rb[g].astype(F32)).astype(BF16)
         e_copy(3, g).start()
 
     def stage_back(g):
-        e_copy(2, g).wait_recv()
-        e_copy(3, g).wait_recv()
+        take(cs.at[g, pl.ds(0, 2)], e_r.at[1, g])
         mine = (po[g, 3] + pr[g, 3].astype(F32) + rc[g].astype(F32) + rd[g].astype(F32)).astype(BF16)
         stacked = jnp.concatenate([mine[:, j * 128 : (j + 1) * 128] for j in range(4)], axis=0)
         rt[pl.ds(m8(g * 8 * MSG, 8 * MSG), 8 * MSG), :] = nn(perm_t[...], stacked).astype(BF16)
@@ -375,10 +368,6 @@
         def _():
             stage_relay(t - 1)
 
-        @pl.when((t >= 2) & (t < GROUPS + 2))
-        def _():
-            stage_far(t - 2)
-
         @pl.when(t == 3)
         def _():
             for copy in loads[5:]:
@@ -389,13 +378,13 @@
             stage_compute(t - 3)
             stage_make(t - 3)
 
+        @pl.when((t >= 2) & (t < GROUPS + 2))
+        def _():
+            stage_far(t - 2)
+
         @pl.when((t >= 4) & (t < GROUPS + 4))
         def _():
             stage_first(t - 4)
-
-        @pl.when(t == GROUPS + 4)
-        def _():
-            lax.fori_loop(0, 4, down_step, 0)
 
         @pl.when((t >= 5) & (t < GROUPS + 5))
         def _():
@@ -416,41 +405,38 @@
     lax.fori_loop(0, 4, up_step, 0)
     own_back.wait()
 
-    def back_wait(p, carry):
-        block = bk.at[pl.ds(m8(p * MSG), MSG), :]
-        rcopy(block, block, rt_s.at[p], rt_r.at[p], mate).wait_recv()
-        return carry
-
-    lax.fori_loop(1, CHIPS, back_wait, 0)
-
+    take(bk.at[pl.ds(0, (CHIPS - 1) * MSG), :], one_r.at[0])
     cols = lax.broadcasted_iota(jnp.int32, (TOK, CHIPS * MSG), 1).astype(F32)
     back = bk[pl.ds(0, CHIPS * MSG), :]
-    for j in range(4):
-        hot = ((cols == s0 + j * CAP) | (cols == s1 + j * CAP)).astype(F32).astype(BF16)
-        dn[:, pl.ds(m8(qcol + j * 128, 128), 128)] = nn(hot, back).astype(BF16)
-
-    def dn_at(off, rows=None):
-        return dn.at[pl.ds(0, TOK) if rows is None else pl.ds(rows, TOK // 2), pl.ds(col(off), Q)]
-
-    def dn_copy(n):
+
+    def dn_at(off, h, rows=None):
+        return dn.at[
+            pl.ds(0, TOK) if rows is None else pl.ds(rows, TOK // 2),
+            pl.ds(m8(((x + off) % NX) * Q + h * 256, 256), 256),
+        ]
+
+    def dn_copy(n, h):
         block, dev = (
-            (dn_at(0), right), (dn_at(0), left), (dn_at(3, 0), right), (dn_at(1, TOK // 2), left)
-        )[n]
-        return rcopy(block, block, dn_s.at[n], dn_r.at[n], dev)
-
-    def dn_wait(n):
-        block = (dn_at(3), dn_at(1), dn_at(2, 0), dn_at(2, TOK // 2))[n]
-        rcopy(block, block, dn_s.at[n], dn_r.at[n], mate).wait_recv()
-
-    dn_copy(0).start()
-    dn_copy(1).start()
+            lambda: (dn_at(0, h), right),
+            lambda: (dn_at(0, h), left),
+            lambda: (dn_at(3, h, 0), right),
+            lambda: (dn_at(1, h, TOK // 2), left),
+        )[n]()
+        return rcopy(block, block, send_sem.at[5], dn_r.at[(0, 2, 4, 4)[n] + (h if n < 2 else 0)], dev)
+
+    for h in range(2):
+        for j in (2 * h, 2 * h + 1):
+            hot = ((cols == s0 + j * CAP) | (cols == s1 + j * CAP)).astype(F32).astype(BF16)
+            dn[:, pl.ds(m8(qcol + j * 128, 128), 128)] = nn(hot, back).astype(BF16)
+        dn_copy(0, h).start()
+        dn_copy(1, h).start()
     mixed = (ogate[...].astype(F32) * cout[...].astype(F32)).astype(BF16)
-    dn_wait(0)
-    dn_copy(2).start()
-    dn_wait(1)
-    dn_copy(3).start()
-    dn_wait(2)
-    dn_wait(3)
+    for h in range(2):
+        take(dn_at(3, h), dn_r.at[h])
+        dn_copy(2, h).start()
+        take(dn_at(1, h), dn_r.at[2 + h])
+        dn_copy(3, h).start()
+    take(dn.at[:, pl.ds(col(2), Q)], dn_r.at[4])
 
     d_norm = dn[...].astype(F32)
     unit = resid[...].astype(F32) * inv
@@ -462,14 +448,18 @@
     gacc[0] = grad_w[:, 0].reshape(CHIPS * 32, C)
     gacc[1] = grad_w[:, 1].reshape(CHIPS * 32, C)
     gb[...] = gacc[1 - k].astype(BF16)
-    gmate = rcopy(gb, gp, t_s.at[0], t_r.at[0], mate)
+    gmate = rcopy(gb, gp, send_sem.at[6], one_r.at[1], mate)
     gmate.start()
 
     d_mix = nt(gr, wout[...])
     d_conv = d_mix * ogate[...].astype(F32)
     dcv[...] = d_conv
-    to_after = rcopy(dcv.at[pl.ds(TOK - 8, 8), :], hp, t_s.at[1], t_r.at[1], after)
-    to_before = rcopy(dcv.at[pl.ds(0, 8), :], hn, t_s.at[2], t_r.at[2], before)
+    to_after = rcopy(
+        dcv.at[pl.ds(TOK - 8, 8), :], halo.at[pl.ds(0, 8), :], send_sem.at[7], one_r.at[2], after
+    )
+    to_before = rcopy(
+        dcv.at[pl.ds(0, 8), :], halo.at[pl.ds(8, 8), :], send_sem.at[7], one_r.at[2], before
+    )
     to_after.start()
     to_before.start()
     gog_o[...] = (d_mix * cout[...].astype(F32)).astype(BF16)
@@ -477,70 +467,59 @@
     gmate.wait_recv()
     gs[...] = (gacc[k] + gp[...].astype(F32)).astype(BF16)
 
-    def g_copy(i, dy):
-        e = expert_of(i, dy)
-        p = place_of(i, dy)
-        return rcopy(
-            gs.at[pl.ds(m8(e * 32, 32), 32), :],
-            g_in.at[pl.ds(p * 32, 32), :],
-            g_s.at[p], g_r.at[p], (2 * e + k, x),
-        )
-
-    for i in range(NZ - 1, -1, -1):
-        for dy in range(NY):
-            if i or dy:
-                g_copy(i, dy).start()
-    own_g = pltpu.make_async_copy(
-        gs.at[pl.ds(m8(c * 32, 32), 32), :], g_in.at[pl.ds(0, 32), :], loc_sem.at[2]
-    )
-    own_g.start()
-
-    to_after.wait_recv()
-    to_before.wait_recv()
+    def gs_block(n, dy):
+        return pl.ds(m8((((z + W_ORDER[n]) % NZ) * NY + (y + dy) % NY) * 32, 32), 32)
+
+    for h in range(2):
+        for n in range(4 * h, 4 * h + 4):
+            for dy in range(1, NY):
+                rcopy(
+                    gs.at[gs_block(n, dy), :],
+                    gy_in.at[pl.ds(((dy - 1) * NZ + n) * 32, 32), :],
+                    send_sem.at[8], g_r.at[h], (2 * (z * NY + (y + dy) % NY) + k, x),
+                ).start()
+
+    lax.fori_loop(0, 4, down_step, 0)
+
+    for h in range(2):
+        take(gy_in.at[pl.ds(0, 384), :], g_r.at[h])
+        near = jnp.concatenate([gs[gs_block(n, 0), :] for n in range(4 * h, 4 * h + 4)], axis=0)
+        total = near.astype(F32)
+        for d in range(NY - 1):
+            total = total + gy_in[d * 256 + h * 128 : d * 256 + (h + 1) * 128, :].astype(F32)
+        gz_out[h * 128 : (h + 1) * 128, :] = total.astype(BF16)
+        for n in range(4 * h, 4 * h + 4):
+            if W_ORDER[n]:
+                rcopy(
+                    gz_out.at[pl.ds(n * 32, 32), :], gz_in.at[pl.ds(n * 32, 32), :],
+                    send_sem.at[9], g_r.at[2],
+                    (2 * (((z + W_ORDER[n]) % NZ) * NY + y) + k, x),
+                ).start()
+    own_sum = total[96:128]
+
+    take(halo, one_r.at[2])
     row = lax.broadcasted_iota(jnp.int32, (TOK, C), 0)
-    next_row = jnp.where(s == 63, 0.0, hn[0:1, :])
-    prev_row = jnp.where(s == 0, 0.0, hp[7:8, :])
+    next_row = jnp.where(s == 63, 0.0, halo[8:9, :])
+    prev_row = jnp.where(s == 0, 0.0, halo[7:8, :])
     nxt = jnp.where(row == TOK - 1, next_row, pltpu.roll(d_conv, TOK - 1, 0))
     prv = jnp.where(row == 0, prev_row, pltpu.roll(d_conv, 1, 0))
     d_inner = taps[0:1, :] * nxt + taps[1:2, :] * d_conv + taps[2:3, :] * prv
     gig_o[...] = (d_inner * cin[...].astype(F32)).astype(BF16)
     gci_o[...] = (d_inner * igate[...].astype(F32)).astype(BF16)
 
-    own_g.wait()
-
-    def g_wait(p, carry):
-        plane_wait(g_in, 32, g_s, g_r, p)
-        return carry
-
-    lax.fori_loop(1, CHIPS, g_wait, 0)
-    gwo_o[...] = jnp.sum(g_in[...].reshape(CHIPS, 32, C).astype(F32), axis=0)
-
-    for i in range(NZ):
-        for dy in range(NY):
-            if i or dy:
-                send_rows(i, dy).wait_send()
-                g_copy(i, dy).wait_send()
-
-    def x_sent(g, carry):
-        for n in range(8):
-            x_copy(n, g).wait_send()
-        mate_copy(g).wait_send()
-        for n in range(4):
-            e_copy(n, g).wait_send()
-        for j in range(8):
-            copy = back_copy(g * 8 + j, source_in(g, j))
-            if j:
-                copy.wait_send()
-            else:
-                pl.when(g > 0)(copy.wait_send)
-        return carry
-
-    lax.fori_loop(0, GROUPS, x_sent, 0)
-    for n in range(4):
-        dn_copy(n).wait_send()
-    gmate.wait_send()
-    to_after.wait_send()
-    to_before.wait_send()
+    take(gz_in.at[pl.ds(0, 224), :], g_r.at[2])
+    gwo_o[...] = own_sum + jnp.sum(gz_in[0:224, :].reshape(7, 32, C).astype(F32), axis=0)
+
+    sent(s_buf.at[pl.ds(0, (CHIPS - 1) * MSG), :], send_sem.at[0])
+    sent(xa.at[:, :, pl.ds(0, 1792)], send_sem.at[1])
+    sent(ps, send_sem.at[2])
+    sent(cs.at[:, pl.ds(0, 3)], send_sem.at[3])
+    sent(rt.at[pl.ds(0, (CHIPS - 1) * MSG), :], send_sem.at[4])
+    sent(dn.at[:, pl.ds(0, 1536)], send_sem.at[5])
+    sent(gb, send_sem.at[6])
+    sent(halo, send_sem.at[7])
+    sent(gy_in, send_sem.at[8])
+    sent(gz_in.at[pl.ds(0, 224), :], send_sem.at[9])
 
 
 def finish(*refs):
@@ -582,11 +561,9 @@
         pltpu.VMEM((slots + 8, 128), BF16), pltpu.VMEM((slots + 8, 128), BF16),
         pltpu.VMEM((TOK, D), BF16),
         pltpu.VMEM((2, 1024, C), F32), pltpu.VMEM((1024, C), BF16), pltpu.VMEM((1024, C), BF16),
-        pltpu.VMEM((1024, C), BF16), pltpu.VMEM((1024, C), BF16),
-        pltpu.VMEM((TOK, C), F32), pltpu.VMEM((8, C), F32), pltpu.VMEM((8, C), F32),
-        dma((15,)), dma((3,)), dma((32,)), dma((32,)), dma((32,)), dma((32,)), dma((32,)), dma((32,)),
-        dma((8, 4)), dma((8, 4)), dma((4,)), dma((4,)), dma((4, 4)), dma((4, 4)), dma((4,)), dma((4,)),
-        dma((3,)), dma((3,)),
+        pltpu.VMEM((1024, C), BF16), pltpu.VMEM((768, C), BF16), pltpu.VMEM((256, C), BF16), pltpu.VMEM((256, C), BF16),
+        pltpu.VMEM((TOK, C), F32), pltpu.VMEM((16, C), F32),
+        dma((15,)), dma((2,)), dma((10,)), dma((4,)), dma((4, 4)), dma((4,)), dma((2, 4)), dma((5,)), dma((3,)), dma((3,)),
     ]
     made = pl.pallas_call(
         kernel,

time: 101 us -> 97.2 us (0.962)
  Pallas kernels: 100 us -> 96.5 us
    pallas_call x1, Pallas kernels: 98.1 us -> 94.2 us  [per_device(): pl.pallas_call(kernel, out_shape=[pltpu.VMEM(*shape) for shape in shapes]...]
where the time goes in v2:
time: 97.2 us; the launch traced here: 97.1 us
  Pallas kernels  96.5 us (99%)
    pallas_call x1, Pallas kernels, per_device(): pl.pallas_call(kernel, out_shape=[pltpu.VMEM(*shape) for shape in shapes]...  94.2 us
    pallas_call x1, Pallas kernels, per_device(): pl.pallas_call(finish, out_shape=[jax.ShapeDtypeStruct(*shape) for shape...  2.29 us

profile of v2, /device:TPU:1, one launch (start us, length us, event | category | flops | bytes accessed | tf_op | source)
XLA Modules:
  0.0 97.1 jit_solution(8254573820560880503)
XLA Ops:
  0.6 94.2 %shard_map.198 = (bf16[128,2048]{1,0:T(8,128)(2,1)S(1)}, bf16[1,2048,512]{2,1,0:T(8,128)(2,1)S(1)}, bf16[1,512,2048]{2,1,0:T(8,128)(2,1)S(1)}, bf16[128,256]{1,0...) custom-call(bf16[128,2048]{1,0:T(8,128)(2,1)} %og_h.1, ...), custom_call_target="tpu_custom_call" | custom-call | tf_op jit(solution)/shard_map/pallas_call | solution.py:568
  94.8 2.3 %shard_map.199 = (bf16[128,2048]{1,0:T(8,128)(2,1)}, bf16[1,2048,512]{2,1,0:T(8,128)(2,1)}, bf16[1,512,2048]{2,1,0:T(8,128)(2,1)}, bf16[128,256]{1,0:T(8,128)(2,...) custom-call(bf16[128,2048]{1,0:T(8,128)(2,1)S(1)} %get-tuple-element.14.refs_0_, ...), custom_call_target="tpu_custom_call" | custom-call | tf_op jit(solution)/shard_map/pallas_call | solution.py:578

commit v3 on v2

--- a/solution.py
+++ b/solution.py
@@ -23,17 +23,16 @@
 GROW = 8 * CAP
 HALF = GROUPS * GROW
 C = 256
-Z_ORDER = (0, 1, 7, 2, 6, 3, 5, 4)
-W_ORDER = (4, 3, 5, 2, 6, 1, 7, 0)
+Z_ORDER = (0, 1, 6, 3, 5, 4, 7, 2)
 O_OFF = (2, 1, 3, 0)
 
 
-def permutation():
-    place = np.zeros((8 * MSG, 8 * MSG), np.float32)
+def permutation(sources):
+    place = np.zeros((sources * MSG, sources * MSG), np.float32)
     for part in range(4):
-        for source in range(8):
+        for source in range(sources):
             for slot in range(CAP):
-                place[part * GROW + source * CAP + slot, source * MSG + part * CAP + slot] = 1
+                place[(part * sources + source) * CAP + slot, source * MSG + part * CAP + slot] = 1
     return place
 
 
@@ -59,8 +58,8 @@
     gr_o, gup_o, gdn_o, gog_o, gig_o, gci_o, gwo_o,
     og, resid, routes, rw, ogate, igate, cin, cout, taps, wout, perm, perm_t,
     wg, wu, wd, s_buf, r_buf, xa, hid, dga, dup, ps, pr, po, ra, rb, rc, rd, cs, rt, bk, dn,
-    gacc, gb, gp, gs, gy_in, gz_out, gz_in, dcv, halo,
-    w_sem, loc_sem, send_sem, pl_r, xr, q_r, e_r, dn_r, g_r, one_r,
+    gacc, gb, gp, gs, gy_in, gz_out, gz_in, dcv, halo, dots,
+    w_sem, loc_sem, send_sem, pl_r, xr, q_r, e_r, dn_r, g_r, one_r, gm_r,
 ):
     s = lax.axis_index("sp")
     x = lax.axis_index("tp")
@@ -70,6 +69,7 @@
     y = c % NY
     right = (s, (x + 1) % NX)
     left = (s, (x + 3) % NX)
+    far = (s, (x + 2) % NX)
     mate = (2 * c + 1 - k, x)
     before = ((s + 63) % 64, x)
     after = ((s + 1) % 64, x)
@@ -93,7 +93,7 @@
                 pl.semaphore_signal(
                     barrier, inc=1, device_id=(2 * expert_of(i, dy) + k, x), device_id_type=MESH
                 )
-    for dev in (right, left, mate, across):
+    for dev in (right, left, far, mate, across):
         pl.semaphore_signal(barrier, inc=1, device_id=dev, device_id_type=MESH)
 
     loads = [
@@ -172,7 +172,7 @@
     lax.fori_loop(0, GROUPS, build, 0)
     loads[4].wait()
 
-    pl.semaphore_wait(barrier, 35)
+    pl.semaphore_wait(barrier, 36)
 
     def send_rows(i, dy):
         e = expert_of(i, dy)
@@ -180,7 +180,7 @@
         return rcopy(
             s_buf.at[pl.ds(m8(e * MSG), MSG), :],
             r_buf.at[pl.ds(p * MSG, MSG), :],
-            send_sem.at[0], pl_r.at[i // 2], (2 * e + k, x),
+            send_sem.at[0], pl_r.at[i], (2 * e + k, x),
         )
 
     own_rows = pltpu.make_async_copy(
@@ -202,18 +202,21 @@
             return xa.at[:, rows, pl.ds(col(off), Q)]
         return xa.at[kind, rows, pl.ds(col(off), Q)]
 
+    def own_copy(n, g, half):
+        block = xa.at[
+            :, pl.ds(m8(k * HALF + g * GROW + half * (GROW // 2)), GROW // 2), pl.ds(qcol, Q)
+        ]
+        return rcopy(block, block, send_sem.at[1], xr.at[(0, 1, 3)[n], g], (right, left, mate)[n])
+
     def x_copy(n, g):
-        block, dev = (
-            (xa_at(k, g, 0), right),
-            (xa_at(k, g, 0), left),
-            (xa_at(k, g, 0), mate),
-            (xa_at(k, g, 3, 0), right),
-            (xa_at(k, g, 1, 1), left),
-            (xa_at(k, g, 3), mate),
-            (xa_at(k, g, 1), mate),
-            (xa_at(k, g, 2), mate),
-        )[n]
-        return rcopy(block, block, send_sem.at[1], xr.at[(0, 1, 3, 2, 2, 3, 3, 3)[n], g], dev)
+        block, dev = {
+            3: lambda: (xa_at(k, g, 3, 0), right),
+            4: lambda: (xa_at(k, g, 1, 1), left),
+            5: lambda: (xa_at(k, g, 3), mate),
+            6: lambda: (xa_at(k, g, 1), mate),
+            7: lambda: (xa_at(k, g, 2), mate),
+        }[n]()
+        return rcopy(block, block, send_sem.at[1], xr.at[2 if n < 5 else 3, g], dev)
 
     def x_wait(n, g):
         block = (
@@ -231,22 +234,28 @@
         rcopy(block, block, sem, sem, mate).wait_send()
 
     def stage_in(g):
-        @pl.when(g == 0)
-        def _():
-            take(r_buf.at[pl.ds(MSG, 7 * MSG), :], pl_r.at[0])
-
-        @pl.when(g > 0)
-        def _():
-            take(r_buf.at[pl.ds(m8(g * 8 * MSG, 8 * MSG), 8 * MSG), :], pl_r.at[g])
-
-        got = nn(perm[...], r_buf[pl.ds(m8(g * 8 * MSG, 8 * MSG), 8 * MSG), :]).astype(BF16)
-        rows = pl.ds(m8(k * HALF + g * GROW, 16), GROW)
-        for kind in range(2):
-            for part in range(2):
-                n = 2 * kind + part
-                xa[kind, rows, pl.ds(m8(qcol + part * 256, 256), 256)] = got[n * GROW : (n + 1) * GROW]
-        for n in (0, 1, 2):
-            x_copy(n, g).start()
+        for half in range(2):
+            base = (2 * g + half) * NY * MSG
+            if half:
+                take(r_buf.at[pl.ds(m8(base, NY * MSG), NY * MSG), :], pl_r.at[2 * g + 1])
+            else:
+
+                @pl.when(g == 0)
+                def _():
+                    take(r_buf.at[pl.ds(MSG, 3 * MSG), :], pl_r.at[0])
+
+                @pl.when(g > 0)
+                def _():
+                    take(r_buf.at[pl.ds(m8(base, NY * MSG), NY * MSG), :], pl_r.at[2 * g])
+
+            got = nn(perm[...], r_buf[pl.ds(m8(base, NY * MSG), NY * MSG), :]).astype(BF16)
+            rows = pl.ds(m8(k * HALF + g * GROW + half * (GROW // 2)), GROW // 2)
+            for kind in range(2):
+                for part in range(2):
+                    n = 2 * kind + part
+                    xa[kind, rows, pl.ds(m8(qcol + part * 256, 256), 256)] = got[n * MSG : (n + 1) * MSG]
+            for n in range(3):
+                own_copy(n, g, half).start()
 
     def stage_relay(g):
         x_wait(0, g)
@@ -303,7 +312,9 @@
         )
 
     def source_in(g, j):
-        away = (NZ - g) % NZ if j < NY else g + 1
+        away = 0
+        for n in range(1 if j < NY else 0, GROUPS):
+            away = away + Z_ORDER[2 * n + j // NY] * (1 - ((g - n) * (g - n) + 8) // 9)
         return ((z + away) % NZ) * NY + (y + j % NY) % NY
 
     def stage_make(g):
@@ -351,12 +362,12 @@
 
     def down_step(b, carry):
         cols = pl.ds(m8(b * 512, 512), 512)
-        gdn_o[0, :, cols] = tn(hid[...], xa[1, :, cols]).astype(BF16)
+        gdn_o[0, :, cols] = tn(hid[...], xa[1, 0 : 2 * HALF, cols]).astype(BF16)
         return carry
 
     def up_step(b, carry):
         cols = pl.ds(m8(b * 512, 512), 512)
-        gup_o[0, cols, :] = tn(xa[0, :, cols], dup[...]).astype(BF16)
+        gup_o[0, cols, :] = tn(xa[0, 0 : 2 * HALF, cols], dup[...]).astype(BF16)
         return carry
 
     def step(t, carry):
@@ -373,12 +384,16 @@
             for copy in loads[5:]:
                 copy.wait()
 
+        @pl.when((t == 2) | ((t >= 4) & (t < GROUPS + 2)))
+        def _():
+            stage_far(t - 2)
+
         @pl.when((t >= 3) & (t < GROUPS + 3))
         def _():
             stage_compute(t - 3)
             stage_make(t - 3)
 
-        @pl.when((t >= 2) & (t < GROUPS + 2))
+        @pl.when(t == 3)
         def _():
             stage_far(t - 2)
 
@@ -424,34 +439,94 @@
         )[n]()
         return rcopy(block, block, send_sem.at[5], dn_r.at[(0, 2, 4, 4)[n] + (h if n < 2 else 0)], dev)
 
+    for j in range(4):
+        hot = ((cols == s0 + j * CAP) | (cols == s1 + j * CAP)).astype(F32).astype(BF16)
+        dn[:, pl.ds(m8(qcol + j * 128, 128), 128)] = nn(hot, back).astype(BF16)
+
+    def unit_of(feats):
+        return resid[:, feats].astype(F32) * inv
+
+    own_feats = pl.ds(qcol, Q)
+    part = jnp.sum(unit_of(own_feats) * dn[:, own_feats].astype(F32), axis=1, keepdims=True)
+    part = jnp.sum(jnp.where(eye, part, 0.0), axis=0, keepdims=True)
+    dots[x] = jnp.broadcast_to(part, (8, TOK))
+    for dev in (right, left, far):
+        rcopy(dots.at[x], dots.at[x], send_sem.at[10], one_r.at[3], dev).start()
     for h in range(2):
-        for j in (2 * h, 2 * h + 1):
-            hot = ((cols == s0 + j * CAP) | (cols == s1 + j * CAP)).astype(F32).astype(BF16)
-            dn[:, pl.ds(m8(qcol + j * 128, 128), 128)] = nn(hot, back).astype(BF16)
         dn_copy(0, h).start()
         dn_copy(1, h).start()
     mixed = (ogate[...].astype(F32) * cout[...].astype(F32)).astype(BF16)
+    take(dots.at[pl.ds(0, 3)], one_r.at[3])
+    means = (dots[0, 0:1, :] + dots[1, 0:1, :] + dots[2, 0:1, :] + dots[3, 0:1, :]) * (1.0 / D)
+    row_mean = jnp.sum(jnp.where(eye, means, 0.0), axis=1, keepdims=True)
+
+    def quarter_rows(off):
+        return pl.ds(m8(((x + off) % NX) * 256, 256), 256)
+
+    def quarter(off, chunk):
+        feats = pl.ds(col(off), Q)
+        rows = quarter_rows(off)
+        gr = (
+            og[:, feats].astype(F32)
+            + inv * (dn[:, feats].astype(F32) - unit_of(feats) * row_mean)
+        ).astype(BF16)
+        gr_o[:, feats] = gr
+        grad_w = tn(gr, mixed).reshape(8, 2, 32, C)
+        gacc[0, rows, :] = grad_w[:, 0].reshape(256, C)
+        gacc[1, rows, :] = grad_w[:, 1].reshape(256, C)
+        gb[rows, :] = gacc[1 - k, rows, :].astype(BF16)
+        rcopy(gb.at[rows, :], gp.at[rows, :], send_sem.at[6], gm_r.at[chunk], mate).start()
+
+    def along_y(offs, first, chunk):
+        for n, off in enumerate(offs):
+            rows = quarter_rows(off)
+            gs[rows, :] = (gacc[k, rows, :] + gp[rows, :].astype(F32)).astype(BF16)
+            for zz in range(2):
+                for dy in range(1, NY):
+                    there = (y + dy) % NY
+                    block = ((2 * ((x + off) % NX) + zz) * NY + there) * 32
+                    rcopy(
+                        gs.at[pl.ds(m8(block, 32), 32), :],
+                        gy_in.at[pl.ds(((dy - 1) * NZ + first + 2 * n + zz) * 32, 32), :],
+                        send_sem.at[8], g_r.at[chunk], (2 * (z * NY + there) + k, x),
+                    ).start()
+
+    def along_z(offs, first):
+        for n, off in enumerate(offs):
+            for zz in range(2):
+                there = 2 * ((x + off) % NX) + zz
+                slot = (first + 2 * n + zz) * 32
+                total = gs[pl.ds(m8((there * NY + y) * 32, 32), 32), :].astype(F32)
+                for d in range(NY - 1):
+                    total = total + gy_in[d * 256 + slot : d * 256 + slot + 32, :].astype(F32)
+                gz_out[slot : slot + 32, :] = total.astype(BF16)
+
+                @pl.when(there == z)
+                def _():
+                    gz_in[pl.ds(m8(z * 32, 32), 32), :] = gz_out[slot : slot + 32, :]
+
+                @pl.when(there != z)
+                def _():
+                    rcopy(
+                        gz_out.at[pl.ds(slot, 32), :], gz_in.at[pl.ds(m8(z * 32, 32), 32), :],
+                        send_sem.at[9], g_r.at[2], (2 * (there * NY + y) + k, x),
+                    ).start()
+
+    near = (0, 3, 1)
+    quarter(0, 0)
     for h in range(2):
         take(dn_at(3, h), dn_r.at[h])
         dn_copy(2, h).start()
         take(dn_at(1, h), dn_r.at[2 + h])
         dn_copy(3, h).start()
+    quarter(3, 0)
+    quarter(1, 0)
+    take(gp.at[pl.ds(0, 768), :], gm_r.at[0])
+    along_y(near, 0, 0)
     take(dn.at[:, pl.ds(col(2), Q)], dn_r.at[4])
-
-    d_norm = dn[...].astype(F32)
-    unit = resid[...].astype(F32) * inv
-    row_mean = jnp.mean(unit * d_norm, axis=-1, keepdims=True)
-    gr = (og[...].astype(F32) + inv * (d_norm - unit * row_mean)).astype(BF16)
-    gr_o[...] = gr
-
-    grad_w = tn(gr, mixed).reshape(CHIPS, 2, 32, C)
-    gacc[0] = grad_w[:, 0].reshape(CHIPS * 32, C)
-    gacc[1] = grad_w[:, 1].reshape(CHIPS * 32, C)
-    gb[...] = gacc[1 - k].astype(BF16)
-    gmate = rcopy(gb, gp, send_sem.at[6], one_r.at[1], mate)
-    gmate.start()
-
-    d_mix = nt(gr, wout[...])
+    quarter(2, 1)
+
+    d_mix = nt(gr_o[...], wout[...])
     d_conv = d_mix * ogate[...].astype(F32)
     dcv[...] = d_conv
     to_after = rcopy(
@@ -464,38 +539,13 @@
     to_before.start()
     gog_o[...] = (d_mix * cout[...].astype(F32)).astype(BF16)
 
-    gmate.wait_recv()
-    gs[...] = (gacc[k] + gp[...].astype(F32)).astype(BF16)
-
-    def gs_block(n, dy):
-        return pl.ds(m8((((z + W_ORDER[n]) % NZ) * NY + (y + dy) % NY) * 32, 32), 32)
-
-    for h in range(2):
-        for n in range(4 * h, 4 * h + 4):
-            for dy in range(1, NY):
-                rcopy(
-                    gs.at[gs_block(n, dy), :],
-                    gy_in.at[pl.ds(((dy - 1) * NZ + n) * 32, 32), :],
-                    send_sem.at[8], g_r.at[h], (2 * (z * NY + (y + dy) % NY) + k, x),
-                ).start()
-
+    take(gp.at[pl.ds(0, 256), :], gm_r.at[1])
+    along_y((2,), 6, 1)
+    take(gy_in.at[pl.ds(0, 576), :], g_r.at[0])
+    along_z(near, 0)
     lax.fori_loop(0, 4, down_step, 0)
-
-    for h in range(2):
-        take(gy_in.at[pl.ds(0, 384), :], g_r.at[h])
-        near = jnp.concatenate([gs[gs_block(n, 0), :] for n in range(4 * h, 4 * h + 4)], axis=0)
-        total = near.astype(F32)
-        for d in range(NY - 1):
-            total = total + gy_in[d * 256 + h * 128 : d * 256 + (h + 1) * 128, :].astype(F32)
-        gz_out[h * 128 : (h + 1) * 128, :] = total.astype(BF16)
-        for n in range(4 * h, 4 * h + 4):
-            if W_ORDER[n]:
-                rcopy(
-                    gz_out.at[pl.ds(n * 32, 32), :], gz_in.at[pl.ds(n * 32, 32), :],
-                    send_sem.at[9], g_r.at[2],
-                    (2 * (((z + W_ORDER[n]) % NZ) * NY + y) + k, x),
-                ).start()
-    own_sum = total[96:128]
+    take(gy_in.at[pl.ds(0, 192), :], g_r.at[1])
+    along_z((2,), 6)
 
     take(halo, one_r.at[2])
     row = lax.broadcasted_iota(jnp.int32, (TOK, C), 0)
@@ -508,10 +558,10 @@
     gci_o[...] = (d_inner * igate[...].astype(F32)).astype(BF16)
 
     take(gz_in.at[pl.ds(0, 224), :], g_r.at[2])
-    gwo_o[...] = own_sum + jnp.sum(gz_in[0:224, :].reshape(7, 32, C).astype(F32), axis=0)
+    gwo_o[...] = jnp.sum(gz_in[...].reshape(NZ, 32, C).astype(F32), axis=0)
 
     sent(s_buf.at[pl.ds(0, (CHIPS - 1) * MSG), :], send_sem.at[0])
-    sent(xa.at[:, :, pl.ds(0, 1792)], send_sem.at[1])
+    sent(xa.at[:, pl.ds(0, 2 * HALF), pl.ds(0, 1792)], send_sem.at[1])
     sent(ps, send_sem.at[2])
     sent(cs.at[:, pl.ds(0, 3)], send_sem.at[3])
     sent(rt.at[pl.ds(0, (CHIPS - 1) * MSG), :], send_sem.at[4])
@@ -520,6 +570,7 @@
     sent(halo, send_sem.at[7])
     sent(gy_in, send_sem.at[8])
     sent(gz_in.at[pl.ds(0, 224), :], send_sem.at[9])
+    sent(dots.at[pl.ds(0, 3)], send_sem.at[10])
 
 
 def finish(*refs):
@@ -532,9 +583,8 @@
 
 
 def per_device(*args):
-    place = permutation()
-    perm = jnp.asarray(place, BF16)
-    perm_t = jnp.asarray(place.T, BF16)
+    perm = jnp.asarray(permutation(NY), BF16)
+    perm_t = jnp.asarray(permutation(8).T, BF16)
     vmem = pl.BlockSpec(memory_space=pltpu.VMEM)
     hbm = pl.BlockSpec(memory_space=pl.ANY)
     dma = pltpu.SemaphoreType.DMA
@@ -548,10 +598,10 @@
         pltpu.VMEM((2, TOK), jnp.int32), pltpu.VMEM((2, TOK), F32),
         pltpu.VMEM((TOK, C), BF16), pltpu.VMEM((TOK, C), BF16), pltpu.VMEM((TOK, C), BF16), pltpu.VMEM((TOK, C), BF16),
         pltpu.VMEM((3, C), F32), pltpu.VMEM((C, D), BF16),
-        pltpu.VMEM((8 * MSG, 8 * MSG), BF16), pltpu.VMEM((8 * MSG, 8 * MSG), BF16),
+        pltpu.VMEM((NY * MSG, NY * MSG), BF16), pltpu.VMEM((8 * MSG, 8 * MSG), BF16),
         pltpu.VMEM((D, H), BF16), pltpu.VMEM((D, H), BF16), pltpu.VMEM((H, D), BF16),
         pltpu.VMEM((slots + 8, 256), BF16), pltpu.VMEM((slots + 8, 256), BF16),
-        pltpu.VMEM((2, 2 * HALF, D), BF16),
+        pltpu.VMEM((2, 2 * HALF + 8, D), BF16),
         pltpu.VMEM((2 * HALF, H), BF16), pltpu.VMEM((2 * HALF, H), BF16), pltpu.VMEM((2 * HALF, H), BF16),
         pltpu.VMEM((GROUPS, 4, GROW, Q), BF16), pltpu.VMEM((GROUPS, 4, GROW, Q), BF16),
         pltpu.VMEM((GROUPS, 4, GROW, Q), F32),
@@ -562,8 +612,8 @@
         pltpu.VMEM((TOK, D), BF16),
         pltpu.VMEM((2, 1024, C), F32), pltpu.VMEM((1024, C), BF16), pltpu.VMEM((1024, C), BF16),
         pltpu.VMEM((1024, C), BF16), pltpu.VMEM((768, C), BF16), pltpu.VMEM((256, C), BF16), pltpu.VMEM((256, C), BF16),
-        pltpu.VMEM((TOK, C), F32), pltpu.VMEM((16, C), F32),
-        dma((15,)), dma((2,)), dma((10,)), dma((4,)), dma((4, 4)), dma((4,)), dma((2, 4)), dma((5,)), dma((3,)), dma((3,)),
+        pltpu.VMEM((TOK, C), F32), pltpu.VMEM((16, C), F32), pltpu.VMEM((NX, 8, TOK), F32),
+        dma((15,)), dma((2,)), dma((11,)), dma((8,)), dma((4, 4)), dma((4,)), dma((2, 4)), dma((5,)), dma((3,)), dma((4,)), dma((2,)),
     ]
     made = pl.pallas_call(
         kernel,

time: 97.2 us -> 89.2 us (0.918)
  Pallas kernels: 96.5 us -> 88.5 us
    pallas_call x1, Pallas kernels: 94.2 us -> 86.2 us  [per_device(): pl.pallas_call(kernel, out_shape=[pltpu.VMEM(*shape) for shape in shapes]...]
where the time goes in v3:
time: 89.2 us; the launch traced here: 89.1 us
  Pallas kernels  88.5 us (99%)
    pallas_call x1, Pallas kernels, per_device(): pl.pallas_call(kernel, out_shape=[pltpu.VMEM(*shape) for shape in shapes]...  86.2 us
    pallas_call x1, Pallas kernels, per_device(): pl.pallas_call(finish, out_shape=[jax.ShapeDtypeStruct(*shape) for shape...  2.29 us

profile of v3, /device:TPU:1, one launch (start us, length us, event | category | flops | bytes accessed | tf_op | source)
XLA Modules:
  0.0 89.1 jit_solution(1737316037421580261)
XLA Ops:
  0.6 86.2 %shard_map.198 = (bf16[128,2048]{1,0:T(8,128)(2,1)S(1)}, bf16[1,2048,512]{2,1,0:T(8,128)(2,1)S(1)}, bf16[1,512,2048]{2,1,0:T(8,128)(2,1)S(1)}, bf16[128,256]{1,0...) custom-call(bf16[128,2048]{1,0:T(8,128)(2,1)} %og_h.1, ...), custom_call_target="tpu_custom_call" | custom-call | tf_op jit(solution)/shard_map/pallas_call | solution.py:618
  86.9 2.3 %shard_map.199 = (bf16[128,2048]{1,0:T(8,128)(2,1)}, bf16[1,2048,512]{2,1,0:T(8,128)(2,1)}, bf16[1,512,2048]{2,1,0:T(8,128)(2,1)}, bf16[128,256]{1,0:T(8,128)(2,...) custom-call(bf16[128,2048]{1,0:T(8,128)(2,1)S(1)} %get-tuple-element.14.refs_0_, ...), custom_call_target="tpu_custom_call" | custom-call | tf_op jit(solution)/shard_map/pallas_call | solution.py:628

commit v4 on v3

--- a/solution.py
+++ b/solution.py
@@ -371,44 +371,28 @@
         return carry
 
     def step(t, carry):
-        @pl.when(t < GROUPS)
-        def _():
-            stage_in(t)
-
-        @pl.when((t >= 1) & (t < GROUPS + 1))
-        def _():
-            stage_relay(t - 1)
-
-        @pl.when(t == 3)
-        def _():
+        def at(cond, stage, *g):
+            pl.when(cond)(lambda: stage(*g))
+
+        def loaded():
             for copy in loads[5:]:
                 copy.wait()
 
-        @pl.when((t == 2) | ((t >= 4) & (t < GROUPS + 2)))
-        def _():
-            stage_far(t - 2)
-
-        @pl.when((t >= 3) & (t < GROUPS + 3))
-        def _():
-            stage_compute(t - 3)
-            stage_make(t - 3)
-
-        @pl.when(t == 3)
-        def _():
-            stage_far(t - 2)
-
-        @pl.when((t >= 4) & (t < GROUPS + 4))
-        def _():
-            stage_first(t - 4)
-
-        @pl.when((t >= 5) & (t < GROUPS + 5))
-        def _():
-            stage_second(t - 5)
-
-        @pl.when(t >= 6)
-        def _():
-            stage_back(t - 6)
-
+        at(t < 4, stage_in, t)
+        at((t >= 1) & (t < 5), stage_relay, t - 1)
+        at(t == 3, loaded)
+        at(t == 4, stage_first, 0)
+        at((t == 2) | (t == 4) | (t == 5), stage_far, t - 2)
+        at(t == 5, stage_second, 0)
+        at((t >= 3) & (t < 7), stage_compute, t - 3)
+        at((t == 5) | (t == 6), stage_first, t - 4)
+        at(t == 6, stage_second, 1)
+        at((t >= 3) & (t < 7), stage_make, t - 3)
+        at(t == 3, stage_far, 1)
+        at(t == 7, stage_back, 0)
+        at(t == 7, stage_first, 3)
+        at((t == 7) | (t == 8), stage_second, t - 5)
+        at(t >= 7, stage_back, t - 6)
         return carry
 
     lax.fori_loop(0, GROUPS + 6, step, 0)
@@ -418,6 +402,7 @@
     )
     own_back.start()
     lax.fori_loop(0, 4, up_step, 0)
+    lax.fori_loop(0, 4, down_step, 0)
     own_back.wait()
 
     take(bk.at[pl.ds(0, (CHIPS - 1) * MSG), :], one_r.at[0])
@@ -543,7 +528,6 @@
     along_y((2,), 6, 1)
     take(gy_in.at[pl.ds(0, 576), :], g_r.at[0])
     along_z(near, 0)
-    lax.fori_loop(0, 4, down_step, 0)
     take(gy_in.at[pl.ds(0, 192), :], g_r.at[1])
     along_z((2,), 6)
 

time: 89.2 us -> 88.3 us (0.990)
  Pallas kernels: 88.5 us -> 87.5 us
    pallas_call x1, Pallas kernels: 86.2 us -> 85.2 us  [per_device(): pl.pallas_call(kernel, out_shape=[pltpu.VMEM(*shape) for shape in shapes]...]
where the time goes in v4:
time: 88.3 us; the launch traced here: 88.2 us
  Pallas kernels  87.5 us (99%)
    pallas_call x1, Pallas kernels, per_device(): pl.pallas_call(kernel, out_shape=[pltpu.VMEM(*shape) for shape in shapes]...  85.2 us
    pallas_call x1, Pallas kernels, per_device(): pl.pallas_call(finish, out_shape=[jax.ShapeDtypeStruct(*shape) for shape...  2.29 us

profile of v4, /device:TPU:1, one launch (start us, length us, event | category | flops | bytes accessed | tf_op | source)
XLA Modules:
  0.0 88.2 jit_solution(6092354901051534142)
XLA Ops:
  0.6 85.2 %shard_map.198 = (bf16[128,2048]{1,0:T(8,128)(2,1)S(1)}, bf16[1,2048,512]{2,1,0:T(8,128)(2,1)S(1)}, bf16[1,512,2048]{2,1,0:T(8,128)(2,1)S(1)}, bf16[128,256]{1,0...) custom-call(bf16[128,2048]{1,0:T(8,128)(2,1)} %og_h.1, ...), custom_call_target="tpu_custom_call" | custom-call | tf_op jit(solution)/shard_map/pallas_call | solution.py:602
  85.9 2.3 %shard_map.199 = (bf16[128,2048]{1,0:T(8,128)(2,1)}, bf16[1,2048,512]{2,1,0:T(8,128)(2,1)}, bf16[1,512,2048]{2,1,0:T(8,128)(2,1)}, bf16[128,256]{1,0:T(8,128)(2,...) custom-call(bf16[128,2048]{1,0:T(8,128)(2,1)S(1)} %get-tuple-element.14.refs_0_, ...), custom_call_target="tpu_custom_call" | custom-call | tf_op jit(solution)/shard_map/pallas_call | solution.py:612

commit v5 on v4

--- a/solution.py
+++ b/solution.py
@@ -188,7 +188,7 @@
     )
     own_rows.start()
     for i in range(NZ):
-        for dy in range(NY):
+        for dy in (2, 1, 3, 0):
             if i or dy:
                 send_rows(i, dy).start()
     own_rows.wait()
@@ -467,7 +467,7 @@
             rows = quarter_rows(off)
             gs[rows, :] = (gacc[k, rows, :] + gp[rows, :].astype(F32)).astype(BF16)
             for zz in range(2):
-                for dy in range(1, NY):
+                for dy in (2, 1, 3):
                     there = (y + dy) % NY
                     block = ((2 * ((x + off) % NX) + zz) * NY + there) * 32
                     rcopy(

time: 88.3 us -> 87.6 us (level)
  no operation moved by 1% of the time
where the time goes in v5:
time: 87.6 us; the launch traced here: 87.5 us
  Pallas kernels  86.9 us (99%)
    pallas_call x1, Pallas kernels, per_device(): pl.pallas_call(kernel, out_shape=[pltpu.VMEM(*shape) for shape in shapes]...  84.6 us
    pallas_call x1, Pallas kernels, per_device(): pl.pallas_call(finish, out_shape=[jax.ShapeDtypeStruct(*shape) for shape...  2.29 us

profile of v5, /device:TPU:1, one launch (start us, length us, event | category | flops | bytes accessed | tf_op | source)
XLA Modules:
  0.0 87.5 jit_solution(9509295404777369277)
XLA Ops:
  0.6 84.6 %shard_map.198 = (bf16[128,2048]{1,0:T(8,128)(2,1)S(1)}, bf16[1,2048,512]{2,1,0:T(8,128)(2,1)S(1)}, bf16[1,512,2048]{2,1,0:T(8,128)(2,1)S(1)}, bf16[128,256]{1,0...) custom-call(bf16[128,2048]{1,0:T(8,128)(2,1)} %og_h.1, ...), custom_call_target="tpu_custom_call" | custom-call | tf_op jit(solution)/shard_map/pallas_call | solution.py:602
  85.2 2.3 %shard_map.199 = (bf16[128,2048]{1,0:T(8,128)(2,1)}, bf16[1,2048,512]{2,1,0:T(8,128)(2,1)}, bf16[1,512,2048]{2,1,0:T(8,128)(2,1)}, bf16[128,256]{1,0:T(8,128)(2,...) custom-call(bf16[128,2048]{1,0:T(8,128)(2,1)S(1)} %get-tuple-element.14.refs_0_, ...), custom_call_target="tpu_custom_call" | custom-call | tf_op jit(solution)/shard_map/pallas_call | solution.py:612
